TPU v7x, 256 devices: a whole 4x4x8 slice. The times are simulated.
256 devices in a mesh: kv: 16 (over y, x), tp: 16 (over z, core).
Axes of the slice: x: 4, y: 4, z: 8, core: 2. Of those that a mesh axis runs over, the one named last changes fastest.
Arguments:
- tokens: bfloat16 [640, 4096], P('tp', 'kv'), may hold values from -8 to 8
- state: float32 [640, 32, 128, 128], P('kv', 'tp'), may hold values from -4 to 4
- mix_gain: float32 [4096], P('kv'), may hold values from 0.1 to 1.9
- q_weight: bfloat16 [4096, 4096], P('kv', 'tp'), may hold values from -0.09375 to 0.09375
- forget_weight: bfloat16 [4096, 4096], P('kv', 'tp'), may hold values from -0.09375 to 0.09375
- input_weight: bfloat16 [4096, 4096], P('kv', 'tp'), may hold values from -0.09375 to 0.09375
- gate_weight: bfloat16 [4096, 4096], P('kv', 'tp'), may hold values from -0.09375 to 0.09375
- lower_bound: float32 [4096], P('tp'), may hold values from 0 to 0.9
- head_gain: float32 [128], replicated, may hold values from 0.1 to 1.9
- out_weight: bfloat16 [4096, 4096], P('tp', 'kv'), may hold values from -0.09375 to 0.09375
- ffn_gain: float32 [4096], P('kv'), may hold values from 0.1 to 1.9
- ffn_gate: bfloat16 [4096, 10240], P('kv', 'tp'), may hold values from -0.09375 to 0.09375
- ffn_up: bfloat16 [4096, 10240], P('kv', 'tp'), may hold values from -0.09375 to 0.09375
- ffn_down: bfloat16 [10240, 4096], P('tp', 'kv'), may hold values from -0.0625 to 0.0625
Outputs:
- layer_out: bfloat16 [640, 4096], P('tp', 'kv')
- new_state: float32 [640, 32, 128, 128], P('kv', 'tp')
All inputs are finite; a program needn't handle non-finite values.
Results may differ from a plain program's by a relative error of at most 0.007.
Values may be sent and summed in bfloat16 or wider, within the bound.
A program may use at most 64 MiB of HBM per device.

v0:
```python
import math

import jax
import jax.numpy as jnp
from jax import lax
from jax.sharding import PartitionSpec as P

EPS = 1e-05


def from_everyone(x, axis):
    copies = jnp.broadcast_to(x, (lax.axis_size(axis), *x.shape))
    return lax.all_to_all(copies, axis, split_axis=0, concat_axis=0, tiled=True)


def in_order(pieces, dim):
    shape = list(pieces.shape[1:])
    shape[dim] *= pieces.shape[0]
    return jnp.moveaxis(pieces, 0, dim).reshape(shape)


def gathered_copies(x, axis, dim):
    pieces = from_everyone(x, axis)
    return in_order(pieces, dim)


def cut_along(x, dim, size):
    shape = x.shape
    pieces = x.reshape(*shape[:dim], size, shape[dim] // size, *shape[dim + 1 :])
    return jnp.moveaxis(pieces, dim, 0)


def sent_and_summed(x, axis, dim):
    size = lax.axis_size(axis)
    pieces = lax.all_to_all(cut_along(x, dim, size), axis, 0, 0, tiled=True)
    return jnp.sum(pieces, axis=0)


def in_one_piece(arrays, axis, dim, along):
    widths = [math.prod(a.shape[along:]) for a in arrays]
    both = jnp.concatenate(
        [a.reshape(*a.shape[:along], w) for a, w in zip(arrays, widths)], axis=along
    )
    out = sent_and_summed(both, axis, dim)
    pieces = jnp.split(out, [sum(widths[:k]) for k in range(1, len(widths))], axis=along)
    return tuple((b.reshape(*out.shape[:along], *a.shape[along:]) for a, b in zip(arrays, pieces)))


def project_in(shard_rows, norm_gain, weight_joined, width):
    rows_all = gathered_copies(shard_rows, "tp", 0)
    values = rows_all.astype(jnp.float32)
    squares = jnp.sum(values * values, axis=1)
    normed = (values * norm_gain).astype(jnp.bfloat16)
    product = jnp.dot(normed, weight_joined, preferred_element_type=jnp.float32)
    sums, totals = in_one_piece((product, squares), "kv", 0, 1)
    sums = sums * lax.rsqrt(totals / width + EPS)[:, None]
    return (rows_all, sums)


def project_back(shard_rows, weight):
    return jnp.dot(gathered_copies(shard_rows, "kv", 0), weight, preferred_element_type=jnp.float32)


def sum_widths(terms):
    return sent_and_summed(terms, "tp", 0)


def body(
    tokens,
    state,
    mix_gain,
    q_weight,
    forget_weight,
    input_weight,
    gate_weight,
    lower_bound,
    head_gain,
    out_weight,
    ffn_gain,
    ffn_gate,
    ffn_up,
    ffn_down,
):
    width = tokens.shape[1] * lax.axis_size("kv")
    mixer_joined = jnp.concatenate((q_weight, forget_weight, input_weight, gate_weight), axis=1)
    ffn_joined = jnp.concatenate((ffn_gate, ffn_up), axis=1)
    whole_tokens, mixer_sums = project_in(tokens, mix_gain, mixer_joined, width)
    head_cols = q_weight.shape[1]
    seq_rows = mixer_sums.shape[0]
    heads_here = state.shape[1]
    head_size = state.shape[2]
    split_shape = (seq_rows, heads_here, head_size)
    query = (jax.nn.silu(mixer_sums[:, :head_cols]) * head_size ** (-0.5)).reshape(split_shape)
    forget = lower_bound + (1.0 - lower_bound) * jax.nn.sigmoid(
        mixer_sums[:, head_cols : 2 * head_cols]
    )
    forget = forget.reshape(split_shape)
    value = mixer_sums[:, 2 * head_cols : 3 * head_cols].reshape(split_shape)
    gate_pre = mixer_sums[:, 3 * head_cols :]
    new_state = forget[..., None] * state + (1.0 - forget)[..., None] * value[:, :, None, :]
    read = jnp.einsum("bhk,bhkv->bhv", query, new_state)
    read = read * lax.rsqrt(jnp.mean(read * read, axis=-1, keepdims=True) + EPS) * head_gain
    gated = (read.reshape(seq_rows, head_cols) * jax.nn.silu(gate_pre)).astype(jnp.bfloat16)
    attended_terms = project_back(gated, out_weight)
    attended = sum_widths(attended_terms)
    own_rows = (tokens.astype(jnp.float32) + attended).astype(jnp.bfloat16)
    unused_rows, ffn_sums = project_in(own_rows, ffn_gain, ffn_joined, width)
    ffn_cols = ffn_gate.shape[1]
    hidden = (jax.nn.silu(ffn_sums[:, :ffn_cols]) * ffn_sums[:, ffn_cols:]).astype(jnp.bfloat16)
    layer_out = (own_rows.astype(jnp.float32) + sum_widths(project_back(hidden, ffn_down))).astype(
        jnp.bfloat16
    )
    return (layer_out, new_state)


def solution(mesh):
    in_specs = (
        P("tp", "kv"),
        P("kv", "tp", None, None),
        P("kv"),
        P("kv", "tp"),
        P("kv", "tp"),
        P("kv", "tp"),
        P("kv", "tp"),
        P("tp"),
        P(),
        P("tp", "kv"),
        P("kv"),
        P("kv", "tp"),
        P("kv", "tp"),
        P("tp", "kv"),
    )
    out_specs = (P("tp", "kv"), P("kv", "tp", None, None))
    return jax.shard_map(body, mesh=mesh, in_specs=in_specs, out_specs=out_specs, check_vma=False)
```

profile of v0, /device:TPU:1, one launch (start us, length us, event | category | flops | bytes accessed | tf_op | source)
XLA Modules:
  0.0 239.3 jit_solution(5957719341241757618)
XLA Ops:
  0.6 0.0 copy-start
  0.6 0.8 broadcast_in_dim.8
  1.4 22.7 %all_to_all.40 = bf16[16,40,256]{2,1,0:T(8,128)(2,1)S(1)} all-to-all(bf16[16,40,256]{2,1,0:T(8,128)(2,1)S(1)} %broadcast_in_dim.8), channel_id=1, replica_groups=mesh['kv'=16,'tp'=16] {'tp'}, dimensions={0} | all-to-all | bytes 655360 | tf_op jit(solution)/shard_map/all_to_all | solution.py:13
  24.2 0.2 fusion.1
  24.3 0.2 copy.30
  24.5 1.6 fusion.7
  26.2 1.8 pad_maximum_fusion.1
  28.0 0.0 copy-start.6
  28.0 6.9 %all-to-all-start.1 = ((f32[16,40,1025]{2,1,0:T(8,128)}), f32[16,40,1025]{2,1,0:T(8,128)S(1)}, u32[]{:S(2)}, u32[]{:S(2)}) async-start(f32[16,40,1025]{2,1,0:T(8,128)} %pad_maximum_fusion.1), calls=%async_computation.1 | async-start | bytes 5898240 | tf_op jit(solution)/shard_map/all_to_all | solution.py:35
  34.9 0.0 copy-done.6
  34.9 46.6 %all-to-all-done.1 = f32[16,40,1025]{2,1,0:T(8,128)S(1)} async-done(((f32[16,40,1025]{2,1,0:T(8,128)}), f32[16,40,1025]{2,1,0:T(8,128)S(1)}, u32[]{:S(2)}, u32[]{:S(2)}) %all-to-all-start.1) | async-done | bytes 2624032 | tf_op jit(solution)/shard_map/all_to_all | solution.py:35
  81.5 0.2 reduce_sum.64
  81.7 0.1 fusion.34
  81.8 0.1 slice_multiply_fusion.1
  82.1 6.6 %multiply_add_fusion = f32[40,2,128,128]{3,2,1,0:T(8,128)S(1)} fusion(f32[40,2,128,128]{3,2,1,0:T(8,128)} %param.15, f32[40,2,128]{2,1,0:T(2,128)S(1)} %mul.136, f32[40,2,128]{2,1,0:T(2,128)S(1)} %broadcast_subtract_fusion, f32[40,2,128]{2,1,0:T(2,128)S(1)} %mul.132), kind=kLoop, calls=%fused_computation | loop fusion | flops 3932160 | bytes 10608640 | tf_op jit(solution)/shard_map/add | solution.py:100
  88.6 0.0 copy-start.1
  88.6 0.0 copy-start.8
  88.7 0.0 copy-start.4
  88.7 0.0 copy-start.5
  88.7 0.8 fusion.37
  89.5 0.0 copy-start.2
  89.5 0.0 copy-start.3
  89.5 0.0 copy-start.7
  89.5 0.1 multiply_reduce_fusion
  89.6 0.0 copy-done.8
  89.6 0.1 multiply_multiply_fusion
  89.8 12.7 %all_to_all.41 = bf16[16,40,256]{2,1,0:T(8,128)(2,1)S(1)} all-to-all(bf16[16,40,256]{2,1,0:T(8,128)(2,1)S(1)} %broadcast_in_dim.9), channel_id=1, replica_groups=mesh['kv'=16,'tp'=16] {'kv'}, dimensions={0} | all-to-all | bytes 655360 | tf_op jit(solution)/shard_map/all_to_all | solution.py:13
  102.5 0.0 copy-done.4
  102.5 0.2 fusion.20
  102.7 0.0 copy-done.1
  102.7 24.6 %all_to_all.42 = f32[16,40,256]{2,1,0:T(8,128)S(1)} all-to-all(f32[16,40,256]{2,1,0:T(8,128)S(1)} %fusion.20), channel_id=1, replica_groups=mesh['kv'=16,'tp'=16] {'tp'}, dimensions={0} | all-to-all | bytes 1310720 | tf_op jit(solution)/shard_map/all_to_all | solution.py:35
  127.4 0.0 copy-done.5
  127.5 15.4 %all_to_all.43 = bf16[16,40,256]{2,1,0:T(8,128)(2,1)S(1)} all-to-all(bf16[16,40,256]{2,1,0:T(8,128)(2,1)S(1)} %broadcast_in_dim.10), channel_id=1, replica_groups=mesh['kv'=16,'tp'=16] {'tp'}, dimensions={0} | all-to-all | bytes 655360 | tf_op jit(solution)/shard_map/all_to_all | solution.py:13
  142.9 0.2 fusion.3
  143.0 0.2 copy.31
  143.2 0.0 copy-done.2
  143.2 0.0 copy-done.3
  143.2 0.0 copy-done.7
  143.3 0.6 fusion.4
  143.9 0.2 pad_maximum_fusion
  144.1 49.7 %all_to_all.44 = f32[16,40,1281]{2,1,0:T(8,128)} all-to-all(f32[16,40,1281]{2,1,0:T(8,128)S(1)} %pad_maximum_fusion), channel_id=1, replica_groups=mesh['kv'=16,'tp'=16] {'kv'}, dimensions={0} | all-to-all | bytes 6558720 | tf_op jit(solution)/shard_map/all_to_all | solution.py:35
  193.8 2.2 reduce_sum.68
  196.1 0.1 fusion.31
  196.2 0.1 slice_multiply_fusion
  196.3 0.1 broadcast_in_dim.11
  196.4 17.5 %all_to_all.45 = bf16[16,40,640]{2,1,0:T(8,128)(2,1)S(1)} all-to-all(bf16[16,40,640]{2,1,0:T(8,128)(2,1)S(1)} %broadcast_in_dim.11), channel_id=1, replica_groups=mesh['kv'=16,'tp'=16] {'kv'}, dimensions={0} | all-to-all | bytes 1638400 | tf_op jit(solution)/shard_map/all_to_all | solution.py:13
  213.9 0.0 copy-done
  213.9 0.4 fusion.16
  214.3 24.3 %all_to_all.46 = f32[16,40,256]{2,1,0:T(8,128)S(1)} all-to-all(f32[16,40,256]{2,1,0:T(8,128)S(1)} %fusion.16), channel_id=1, replica_groups=mesh['kv'=16,'tp'=16] {'tp'}, dimensions={0} | all-to-all | bytes 1310720 | tf_op jit(solution)/shard_map/all_to_all | solution.py:35
  238.7 0.6 add_convert_fusion
  (14 shorter events, 0.3 us)
Async XLA Ops:
  0.6 213.2 %copy-start = (bf16[640,256]{1,0:T(8,128)(2,1)S(1)}, bf16[640,256]{1,0:T(8,128)(2,1)}, u32[]{:S(2)}) copy-start(bf16[640,256]{1,0:T(8,128)(2,1)} %param.27) | copy-start | bytes 983044
  28.0 6.9 %copy-start.6 = (f32[256]{0:T(256)S(1)}, f32[256]{0:T(256)}, u32[]{:S(2)}) copy-start(f32[256]{0:T(256)} %param.21) | copy-start | bytes 3076
  28.0 53.5 %all-to-all-start.1 = ((f32[16,40,1025]{2,1,0:T(8,128)}), f32[16,40,1025]{2,1,0:T(8,128)S(1)}, u32[]{:S(2)}, u32[]{:S(2)}) async-start(f32[16,40,1025]{2,1,0:T(8,128)} %pad_maximum_fusion.1), calls=%async_computation.1 | async-start | bytes 5898240 | tf_op jit(solution)/shard_map/all_to_all | solution.py:35
  88.6 14.1 %copy-start.1 = (f32[40,2,128,128]{3,2,1,0:T(8,128)}, f32[40,2,128,128]{3,2,1,0:T(8,128)S(1)}, u32[]{:S(2)}) copy-start(f32[40,2,128,128]{3,2,1,0:T(8,128)S(1)} %multiply_add_fusion) | copy-start | bytes 15728644
  88.6 1.0 copy-start.8
  88.7 13.8 %copy-start.4 = (bf16[256,256]{1,0:T(8,128)(2,1)S(1)}, bf16[256,256]{1,0:T(8,128)(2,1)}, u32[]{:S(2)}) copy-start(bf16[256,256]{1,0:T(8,128)(2,1)} %param.23) | copy-start | bytes 393220
  88.7 38.7 %copy-start.5 = (bf16[40,256]{1,0:T(8,128)(2,1)S(1)}, bf16[40,256]{1,0:T(8,128)(2,1)}, u32[]{:S(2)}) copy-start(bf16[40,256]{1,0:T(8,128)(2,1)} %param.14) | copy-start | bytes 61444
  89.5 53.7 %copy-start.2 = (bf16[256,640]{1,0:T(8,128)(2,1)S(1)}, bf16[256,640]{1,0:T(8,128)(2,1)}, u32[]{:S(2)}) copy-start(bf16[256,640]{1,0:T(8,128)(2,1)} %param.26) | copy-start | bytes 983044
  89.5 53.8 %copy-start.3 = (bf16[256,640]{1,0:T(8,128)(2,1)S(1)}, bf16[256,640]{1,0:T(8,128)(2,1)}, u32[]{:S(2)}) copy-start(bf16[256,640]{1,0:T(8,128)(2,1)} %param.25) | copy-start | bytes 983044
  89.5 53.8 %copy-start.7 = (f32[256]{0:T(256)S(1)}, f32[256]{0:T(256)}, u32[]{:S(2)}) copy-start(f32[256]{0:T(256)} %param.24) | copy-start | bytes 3076
where the time goes:
time: 240 us; the launch traced here: 239 us
  blocking collectives  167 us (70%)
  waiting for transfers between devices  46.6 us (19%)
  other arithmetic  12.8 us (5%)
  starting transfers between devices  6.88 us (3%)
  matrix products  3.7 us (2%)
    all_to_all x3, blocking collectives, sent_and_summed(): pieces = lax.all_to_all(cut_along(x, dim, size), axis, 0, 0, tiled=True)  98.7 us
    all_to_all x4, blocking collectives, from_everyone(): return lax.all_to_all(copies, axis, split_axis=0, concat_axis=0, tiled=True)  68.3 us
    all_to_all x1, waiting for transfers between devices, sent_and_summed(): pieces = lax.all_to_all(cut_along(x, dim, size), axis, 0, 0, tiled=True)  46.6 us
    all_to_all x1, starting transfers between devices, sent_and_summed(): pieces = lax.all_to_all(cut_along(x, dim, size), axis, 0, 0, tiled=True)  6.88 us
    add x1, other arithmetic, body(): forget[..., None] * state + (1.0 - forget)[..., None] * value[:, :, None, :]  6.56 us
  transfers between devices with their start and end apart: 1, of which 1 were waited for; matrix products, arithmetic and copies ran while one was open for 0% of the time, Pallas kernels for 0%

commit v1 on v0

--- a/solution.py
+++ b/solution.py
@@ -32,8 +32,8 @@
 
 def sent_and_summed(x, axis, dim):
     size = lax.axis_size(axis)
-    pieces = lax.all_to_all(cut_along(x, dim, size), axis, 0, 0, tiled=True)
-    return jnp.sum(pieces, axis=0)
+    pieces = lax.all_to_all(cut_along(x.astype(jnp.bfloat16), dim, size), axis, 0, 0, tiled=True)
+    return jnp.sum(pieces.astype(jnp.float32), axis=0)
 
 
 def in_one_piece(arrays, axis, dim, along):

time: 240 us -> 180 us (0.75)
  blocking collectives: 167 us -> 129 us
  waiting for transfers between devices: 46.6 us -> 25.6 us
  other arithmetic: 12.8 us -> 10.3 us
    all_to_all x3, blocking collectives: 98.7 us -> 63.3 us  [sent_and_summed(): lax.all_to_all(cut_along(x.astype(jnp.bfloat16), dim, size), axis, 0, 0,...]
    all_to_all x1, waiting for transfers between devices: 46.6 us -> 25.6 us  [sent_and_summed(): lax.all_to_all(cut_along(x.astype(jnp.bfloat16), dim, size), axis, 0, 0,...]
where the time goes in v1:
time: 180 us
  blocking collectives  129 us (72%)
  waiting for transfers between devices  25.6 us (14%)
  other arithmetic  10.3 us (6%)
  starting transfers between devices  6.76 us (4%)
  matrix products  3.68 us (2%)
  local copies, waits for them, and re-layouts  2.98 us (2%)
    all_to_all x4, blocking collectives, from_everyone(): return lax.all_to_all(copies, axis, split_axis=0, concat_axis=0, tiled=True)  66 us
    all_to_all x3, blocking collectives, sent_and_summed(): lax.all_to_all(cut_along(x.astype(jnp.bfloat16), dim, size), axis, 0, 0,...  63.3 us
    all_to_all x1, waiting for transfers between devices, sent_and_summed(): lax.all_to_all(cut_along(x.astype(jnp.bfloat16), dim, size), axis, 0, 0,...  25.6 us
    all_to_all x1, starting transfers between devices, sent_and_summed(): lax.all_to_all(cut_along(x.astype(jnp.bfloat16), dim, size), axis, 0, 0,...  6.76 us
    add x1, other arithmetic, body(): forget[..., None] * state + (1.0 - forget)[..., None] * value[:, :, None, :]  6.56 us
  transfers between devices with their start and end apart: 1, of which 1 were waited for; matrix products, arithmetic and copies ran while one was open for 0% of the time, Pallas kernels for 0%

profile of v1, /device:TPU:1, one launch (start us, length us, event | category | flops | bytes accessed | tf_op | source)
XLA Modules:
  0.0 179.5 jit_solution(11956863464606525029)
XLA Ops:
  0.6 0.0 copy-start
  0.6 0.8 broadcast_in_dim.8
  1.4 22.7 %all_to_all.40 = bf16[16,40,256]{2,1,0:T(8,128)(2,1)S(1)} all-to-all(bf16[16,40,256]{2,1,0:T(8,128)(2,1)S(1)} %broadcast_in_dim.8), channel_id=1, replica_groups=mesh['kv'=16,'tp'=16] {'tp'}, dimensions={0} | all-to-all | bytes 655360 | tf_op jit(solution)/shard_map/all_to_all | solution.py:13
  24.2 0.2 fusion.1
  24.3 0.2 copy.30
  24.6 1.6 convolution_convert_fusion.1
  26.2 0.0 copy-start.6
  26.2 1.2 pad_maximum_fusion.1
  27.4 6.8 %all-to-all-start.1 = ((bf16[16,40,1025]{2,1,0:T(8,128)(2,1)}), bf16[16,40,1025]{2,1,0:T(8,128)(2,1)S(1)}, u32[]{:S(2)}, u32[]{:S(2)}) async-start(bf16[16,40,1025]{2,1,0:T(8,128)(2,1)} %pad_maximum_fusion.1), calls=%async_computation.1 | async-start | bytes 2949120 | tf_op jit(solution)/shard_map/all_to_all | solution.py:35
  34.2 0.0 copy-done.6
  34.2 25.6 %all-to-all-done.1 = bf16[16,40,1025]{2,1,0:T(8,128)(2,1)S(1)} async-done(((bf16[16,40,1025]{2,1,0:T(8,128)(2,1)}), bf16[16,40,1025]{2,1,0:T(8,128)(2,1)S(1)}, u32[]{:S(2)}, u32[]{:S(2)}) %all-to-all-start.1) | async-done | bytes 1312032 | tf_op jit(solution)/shard_map/all_to_all | solution.py:35
  59.8 0.2 convert_reduce_fusion.1
  60.0 0.1 fusion.28
  60.1 0.1 slice_multiply_fusion.1
  60.4 6.6 %multiply_add_fusion = f32[40,2,128,128]{3,2,1,0:T(8,128)S(1)} fusion(f32[40,2,128,128]{3,2,1,0:T(8,128)} %param.15, f32[40,2,128]{2,1,0:T(2,128)S(1)} %mul.136, f32[40,2,128]{2,1,0:T(2,128)S(1)} %broadcast_subtract_fusion, f32[40,2,128]{2,1,0:T(2,128)S(1)} %mul.132), kind=kLoop, calls=%fused_computation | loop fusion | flops 3932160 | bytes 10608640 | tf_op jit(solution)/shard_map/add | solution.py:100
  67.0 0.0 copy-start.1
  67.0 0.0 copy-start.8
  67.0 0.0 copy-start.4
  67.0 0.8 fusion.31
  67.8 1.5 copy-done.1
  69.3 0.0 copy-start.5
  69.3 0.0 copy-start.2
  69.3 0.0 copy-start.3
  69.3 0.0 copy-start.7
  69.3 0.1 multiply_reduce_fusion
  69.5 0.0 copy-done.8
  69.5 0.1 multiply_multiply_fusion
  69.7 11.4 %all_to_all.41 = bf16[16,40,256]{2,1,0:T(8,128)(2,1)S(1)} all-to-all(bf16[16,40,256]{2,1,0:T(8,128)(2,1)S(1)} %broadcast_in_dim.9), channel_id=1, replica_groups=mesh['kv'=16,'tp'=16] {'kv'}, dimensions={0} | all-to-all | bytes 655360 | tf_op jit(solution)/shard_map/all_to_all | solution.py:13
  81.0 0.0 copy-done.4
  81.0 0.2 convolution_convert_fusion.3
  81.3 17.3 %all_to_all.42 = bf16[16,40,256]{2,1,0:T(8,128)(2,1)S(1)} all-to-all(bf16[16,40,256]{2,1,0:T(8,128)(2,1)S(1)} %bitcast.32), channel_id=1, replica_groups=mesh['kv'=16,'tp'=16] {'tp'}, dimensions={0} | all-to-all | bytes 655360 | tf_op jit(solution)/shard_map/all_to_all | solution.py:35
  98.5 0.1 convert_reduce_fusion.3
  98.6 0.0 copy-done.5
  98.6 15.5 %all_to_all.43 = bf16[16,40,256]{2,1,0:T(8,128)(2,1)S(1)} all-to-all(bf16[16,40,256]{2,1,0:T(8,128)(2,1)S(1)} %broadcast_in_dim.10), channel_id=1, replica_groups=mesh['kv'=16,'tp'=16] {'tp'}, dimensions={0} | all-to-all | bytes 655360 | tf_op jit(solution)/shard_map/all_to_all | solution.py:13
  114.2 0.2 fusion.3
  114.3 0.2 copy.31
  114.5 0.0 copy-done.2
  114.6 0.0 copy-done.3
  114.6 0.0 copy-done.7
  114.6 0.6 convolution_convert_fusion
  115.2 0.1 pad_maximum_fusion
  115.3 28.5 %all_to_all.44 = bf16[16,40,1281]{2,1,0:T(8,128)(2,1)S(1)} all-to-all(bf16[16,40,1281]{2,1,0:T(8,128)(2,1)S(1)} %pad_maximum_fusion), channel_id=1, replica_groups=mesh['kv'=16,'tp'=16] {'kv'}, dimensions={0} | all-to-all | bytes 3279360 | tf_op jit(solution)/shard_map/all_to_all | solution.py:35
  143.8 0.3 convert_reduce_fusion
  144.1 0.1 fusion.25
  144.2 0.1 slice_multiply_fusion
  144.4 0.1 broadcast_in_dim.11
  144.4 16.4 %all_to_all.45 = bf16[16,40,640]{2,1,0:T(8,128)(2,1)S(1)} all-to-all(bf16[16,40,640]{2,1,0:T(8,128)(2,1)S(1)} %broadcast_in_dim.11), channel_id=1, replica_groups=mesh['kv'=16,'tp'=16] {'kv'}, dimensions={0} | all-to-all | bytes 1638400 | tf_op jit(solution)/shard_map/all_to_all | solution.py:13
  160.9 0.0 copy-done
  160.9 0.4 convolution_convert_fusion.2
  161.3 17.6 %all_to_all.46 = bf16[16,40,256]{2,1,0:T(8,128)(2,1)S(1)} all-to-all(bf16[16,40,256]{2,1,0:T(8,128)(2,1)S(1)} %bitcast.33), channel_id=1, replica_groups=mesh['kv'=16,'tp'=16] {'tp'}, dimensions={0} | all-to-all | bytes 655360 | tf_op jit(solution)/shard_map/all_to_all | solution.py:35
  178.9 0.1 convert_reduce_fusion.2
  178.9 0.6 add_convert_fusion
  (12 shorter events, 0.3 us)
Async XLA Ops:
  0.6 160.2 %copy-start = (bf16[640,256]{1,0:T(8,128)(2,1)S(1)}, bf16[640,256]{1,0:T(8,128)(2,1)}, u32[]{:S(2)}) copy-start(bf16[640,256]{1,0:T(8,128)(2,1)} %param.27) | copy-start | bytes 983044
  26.2 8.0 %copy-start.6 = (f32[256]{0:T(256)S(1)}, f32[256]{0:T(256)}, u32[]{:S(2)}) copy-start(f32[256]{0:T(256)} %param.21) | copy-start | bytes 3076
  27.4 32.3 %all-to-all-start.1 = ((bf16[16,40,1025]{2,1,0:T(8,128)(2,1)}), bf16[16,40,1025]{2,1,0:T(8,128)(2,1)S(1)}, u32[]{:S(2)}, u32[]{:S(2)}) async-start(bf16[16,40,1025]{2,1,0:T(8,128)(2,1)} %pad_maximum_fusion.1), calls=%async_computation.1 | async-start | bytes 2949120 | tf_op jit(solution)/shard_map/all_to_all | solution.py:35
  67.0 2.4 %copy-start.1 = (f32[40,2,128,128]{3,2,1,0:T(8,128)}, f32[40,2,128,128]{3,2,1,0:T(8,128)S(1)}, u32[]{:S(2)}) copy-start(f32[40,2,128,128]{3,2,1,0:T(8,128)S(1)} %multiply_add_fusion) | copy-start | bytes 15728644
  67.0 2.5 %copy-start.8 = (f32[128]{0:T(128)S(1)}, f32[128]{0:T(128)}, u32[]{:S(2)}) copy-start(f32[128]{0:T(128)} %param.22) | copy-start | bytes 1540
  67.0 14.0 %copy-start.4 = (bf16[256,256]{1,0:T(8,128)(2,1)S(1)}, bf16[256,256]{1,0:T(8,128)(2,1)}, u32[]{:S(2)}) copy-start(bf16[256,256]{1,0:T(8,128)(2,1)} %param.23) | copy-start | bytes 393220
  69.3 29.3 %copy-start.5 = (bf16[40,256]{1,0:T(8,128)(2,1)S(1)}, bf16[40,256]{1,0:T(8,128)(2,1)}, u32[]{:S(2)}) copy-start(bf16[40,256]{1,0:T(8,128)(2,1)} %param.14) | copy-start | bytes 61444
  69.3 45.2 %copy-start.2 = (bf16[256,640]{1,0:T(8,128)(2,1)S(1)}, bf16[256,640]{1,0:T(8,128)(2,1)}, u32[]{:S(2)}) copy-start(bf16[256,640]{1,0:T(8,128)(2,1)} %param.26) | copy-start | bytes 983044
  69.3 45.2 %copy-start.3 = (bf16[256,640]{1,0:T(8,128)(2,1)S(1)}, bf16[256,640]{1,0:T(8,128)(2,1)}, u32[]{:S(2)}) copy-start(bf16[256,640]{1,0:T(8,128)(2,1)} %param.25) | copy-start | bytes 983044
  69.3 45.2 %copy-start.7 = (f32[256]{0:T(256)S(1)}, f32[256]{0:T(256)}, u32[]{:S(2)}) copy-start(f32[256]{0:T(256)} %param.24) | copy-start | bytes 3076

commit v2 on v1

v2 whole, which is shorter than its diff:
```python
import functools

import jax
import jax.numpy as jnp
from jax import lax
from jax.experimental import pallas as pl
from jax.experimental.pallas import tpu as pltpu
from jax.sharding import PartitionSpec as P

EPS = 1e-05
MESH = pl.DeviceIdType.MESH
F32 = jnp.float32
BF16 = jnp.bfloat16


def layer(
    n,
    nx,
    nz,
    width,
    tokens,
    state_in,
    mix_gain,
    lower_bound,
    head_gain,
    ffn_gain,
    wq_in,
    wf_in,
    wi_in,
    wg_in,
    wo_in,
    wfg_in,
    wfu_in,
    wfd_in,
    out,
    state_out,
    w_mix,
    w_out,
    w_ffn,
    w_down,
    state,
    x1,
    s2,
    r2,
    sq_s2,
    sq_r2,
    acc2,
    read_rows,
    gated,
    g3,
    s4,
    r4,
    own,
    x5,
    s6,
    r6,
    sq_s6,
    sq_r6,
    acc6,
    hidden,
    h7,
    s8,
    r8,
    w_sem,
    st_sem,
    so_sem,
    send_sem,
    sq_send_sem,
    x1_sem,
    r2_sem,
    q2_sem,
    g3_sem,
    r4_sem,
    x5_sem,
    r6_sem,
    q6_sem,
    h7_sem,
    r8_sem,
):
    kv = lax.axis_index("kv")
    tp = lax.axis_index("tp")
    ny = n // nx
    rows, cols = tokens.shape
    heads, head = state.shape[1], state.shape[2]

    def kv_peer(j):
        x = (kv % nx + nx // 2 + nx - j % nx) % nx
        y = (kv // nx + ny // 2 + ny - j // nx) % ny
        return y * nx + x

    def tp_peer(j):
        z = (tp // 2 + nz // 2 + nz - j // 2) % nz
        core = (tp % 2 + 1 + j) % 2
        return z * 2 + core

    def kv_source(j):
        x = (kv % nx + nx // 2 + j % nx) % nx
        y = (kv // nx + ny // 2 + j // nx) % ny
        return y * nx + x

    def tp_source(j):
        z = (tp // 2 + nz // 2 + j // 2) % nz
        core = (tp % 2 + 1 + j) % 2
        return z * 2 + core

    axes = {
        "kv": (kv, kv_peer, kv_source, lambda p: (p, tp)),
        "tp": (tp, tp_peer, tp_source, lambda p: (kv, p)),
    }

    def loop(body):
        lax.fori_loop(0, n, lambda j, c: (body(j), c)[1], 0)

    barrier = pltpu.get_barrier_semaphore()

    def greet(j):
        for me, peer_of, _, place in axes.values():
            peer = peer_of(j)

            @pl.when(peer != me)
            def _():
                pl.semaphore_signal(
                    barrier, inc=1, device_id=place(peer), device_id_type=MESH
                )

    loop(greet)

    side = wq_in.shape[1]
    up = wfg_in.shape[1]
    loads = [
        (wq_in, w_mix.at[:, pl.ds(0, side)]),
        (wf_in, w_mix.at[:, pl.ds(side, side)]),
        (wi_in, w_mix.at[:, pl.ds(2 * side, side)]),
        (wg_in, w_mix.at[:, pl.ds(3 * side, side)]),
        (wo_in, w_out),
        (wfg_in, w_ffn.at[:, pl.ds(0, up)]),
        (wfu_in, w_ffn.at[:, pl.ds(up, up)]),
        (wfd_in, w_down),
    ]
    loads = [pltpu.make_async_copy(a, b, w_sem.at[i]) for i, (a, b) in enumerate(loads)]
    for copy in loads:
        copy.start()
    state_load = pltpu.make_async_copy(state_in, state, st_sem)
    state_load.start()

    pl.semaphore_wait(barrier, 2 * (n - 1))

    def send(axis, source, target, phase_sem, recv_sem, peer):
        me, _, _, place = axes[axis]

        @pl.when(peer != me)
        def _():
            pltpu.make_async_remote_copy(
                src_ref=source,
                dst_ref=target.at[me],
                send_sem=phase_sem,
                recv_sem=recv_sem.at[me],
                device_id=place(peer),
                device_id_type=MESH,
            ).start()

        @pl.when(peer == me)
        def _():
            pltpu.make_async_copy(source, target.at[me], recv_sem.at[me]).start()

    def arrived(target, recv_sem, who):
        pltpu.make_async_copy(target.at[who], target.at[who], recv_sem.at[who]).wait()

    def gather(axis, source, target, phase, recv_sem):
        peer_of = axes[axis][1]
        loop(lambda j: send(axis, source, target, send_sem.at[phase], recv_sem, peer_of(j)))

    def add_up(axis, target, recv_sem, total):
        source_of = axes[axis][2]
        total[...] = jnp.zeros_like(total)

        def step(j):
            who = source_of(j)
            arrived(target, recv_sem, who)
            total[...] += target[who].astype(F32)

        loop(step)

    def projected(x, x_sem, gain, weight, s, r, r_sem, sq_s, sq_r, q_sem, phase):
        ones = jnp.ones((8, cols), F32)

        def step(j):
            who = kv_peer(j)
            arrived(x, x_sem, who)
            values = x[who].astype(F32)
            normed = (values * gain[...]).astype(BF16)
            s[who] = jnp.dot(normed, weight[...], preferred_element_type=F32).astype(BF16)
            send("kv", s.at[who], r, send_sem.at[phase], r_sem, who)
            squares = lax.dot_general(
                ones,
                values * values,
                (((1,), (1,)), ((), ())),
                precision=lax.Precision.HIGHEST,
                preferred_element_type=F32,
            )
            sq_s[who, :, pl.ds(0, rows)] = squares[0:1]
            send("kv", sq_s.at[who], sq_r, sq_send_sem.at[phase], q_sem, who)

        sq_s[...] = jnp.zeros_like(sq_s)
        loop(step)

    def factor(sq_r, q_sem):
        def step(j, total):
            who = kv_source(j)
            arrived(sq_r, q_sem, who)
            return total + sq_r[who]

        total = lax.fori_loop(0, n, step, jnp.zeros((1, 128), F32))
        row = lax.rsqrt(total * (1.0 / width) + EPS)
        return jnp.transpose(jnp.broadcast_to(row, (128, 128)))[0:rows]

    def back(g, g_sem, weight, s, r, r_sem, phase):
        def step(j):
            who = tp_peer(j)
            arrived(g, g_sem, who)
            s[who] = jnp.dot(g[who], weight[...], preferred_element_type=F32).astype(BF16)
            send("tp", s.at[who], r, send_sem.at[phase], r_sem, who)

        loop(step)

    gather("tp", tokens, x1, 0, x1_sem)
    for copy in loads[0:4]:
        copy.wait()
    projected(x1, x1_sem, mix_gain, w_mix, s2, r2, r2_sem, sq_s2, sq_r2, q2_sem, 1)
    add_up("kv", r2, r2_sem, acc2)
    scale = factor(sq_r2, q2_sem)

    state_load.wait()
    for h in range(heads):
        q_at = pl.ds(h * head, head)
        f_at = pl.ds(side + h * head, head)
        v_at = pl.ds(2 * side + h * head, head)
        query_pre = acc2[:, q_at] * scale
        acc2[:, q_at] = query_pre * jax.nn.sigmoid(query_pre) * (head ** (-0.5))
        low = lower_bound[:, q_at]
        acc2[:, f_at] = low + (1.0 - low) * jax.nn.sigmoid(acc2[:, f_at] * scale)
        acc2[:, v_at] = acc2[:, v_at] * scale

    def state_out_copy(group):
        at = pl.ds(group * 8, 8)
        return pltpu.make_async_copy(state.at[at], state_out.at[at], so_sem)

    def eight(group, carry):
        first = pl.multiple_of(group * 8, 8)
        for h in range(heads):
            eight_rows = pl.ds(first, 8)
            query = jnp.transpose(acc2[eight_rows, pl.ds(h * head, head)])
            forget = jnp.transpose(acc2[eight_rows, pl.ds(side + h * head, head)])
            value = acc2[eight_rows, pl.ds(2 * side + h * head, head)]
            reads = []
            for b in range(8):
                v = value[b : b + 1]
                new = v + forget[:, b : b + 1] * (state[first + b, h] - v)
                state[first + b, h] = new
                reads.append(jnp.sum(query[:, b : b + 1] * new, axis=0, keepdims=True))
            read_rows[eight_rows, pl.ds(h * head, head)] = jnp.concatenate(reads, axis=0)
        state_out_copy(group).start()
        return carry

    lax.fori_loop(0, rows // 8, eight, 0)

    for h in range(heads):
        at = pl.ds(h * head, head)
        read = read_rows[:, at]
        mean = jnp.mean(read * read, axis=-1, keepdims=True)
        read = read * lax.rsqrt(mean + EPS) * head_gain[...]
        gate = acc2[:, pl.ds(3 * side + h * head, head)] * scale
        gated[:, at] = (read * (gate * jax.nn.sigmoid(gate))).astype(BF16)

    gather("kv", gated, g3, 2, g3_sem)
    loads[4].wait()
    back(g3, g3_sem, w_out, s4, r4, r4_sem, 3)
    add_up("tp", r4, r4_sem, read_rows)
    own[...] = (tokens[...].astype(F32) + read_rows[...]).astype(BF16)

    gather("tp", own, x5, 4, x5_sem)
    loads[5].wait()
    loads[6].wait()
    projected(x5, x5_sem, ffn_gain, w_ffn, s6, r6, r6_sem, sq_s6, sq_r6, q6_sem, 5)
    add_up("kv", r6, r6_sem, acc6)
    scale = factor(sq_r6, q6_sem)
    for c in range(up // 128):
        at = pl.ds(c * 128, 128)
        gate = acc6[:, at] * scale
        hidden[:, at] = (
            gate * jax.nn.sigmoid(gate) * (acc6[:, pl.ds(up + c * 128, 128)] * scale)
        ).astype(BF16)
    gather("kv", hidden, h7, 6, h7_sem)
    loads[7].wait()
    back(h7, h7_sem, w_down, s8, r8, r8_sem, 7)
    add_up("tp", r8, r8_sem, read_rows)
    out[...] = (own[...].astype(F32) + read_rows[...]).astype(BF16)

    for phase, buffer in enumerate((x1, r2, g3, r4, x5, r6, h7, r8)):
        sent = buffer.at[pl.ds(0, n - 1)]
        pltpu.make_async_copy(sent, sent, send_sem.at[phase]).wait()
    for phase, buffer in ((1, sq_r2), (5, sq_r6)):
        sent = buffer.at[pl.ds(0, n - 1)]
        pltpu.make_async_copy(sent, sent, sq_send_sem.at[phase]).wait()
    pltpu.make_async_copy(state, state_out, so_sem).wait()


def body(
    tokens,
    state,
    mix_gain,
    q_weight,
    forget_weight,
    input_weight,
    gate_weight,
    lower_bound,
    head_gain,
    out_weight,
    ffn_gain,
    ffn_gate,
    ffn_up,
    ffn_down,
):
    n = lax.axis_size("kv")
    nx, nz = {16: (4, 8), 4: (2, 2)}[n]
    rows, cols = tokens.shape
    side, up = q_weight.shape[1], ffn_gate.shape[1]
    vmem, dma = pltpu.VMEM, pltpu.SemaphoreType.DMA
    in_vmem = pl.BlockSpec(memory_space=pltpu.VMEM)
    in_hbm = pl.BlockSpec(memory_space=pl.ANY)
    narrow = (n, rows, cols)
    return pl.pallas_call(
        functools.partial(layer, n, nx, nz, cols * n),
        out_shape=(
            jax.ShapeDtypeStruct(tokens.shape, BF16),
            jax.ShapeDtypeStruct(state.shape, F32),
        ),
        in_specs=[in_vmem, in_hbm, in_vmem, in_vmem, in_vmem, in_vmem] + [in_hbm] * 8,
        out_specs=(in_vmem, in_hbm),
        scratch_shapes=[
            vmem((cols, 4 * side), BF16),
            vmem(out_weight.shape, BF16),
            vmem((cols, 2 * up), BF16),
            vmem(ffn_down.shape, BF16),
            vmem(state.shape, F32),
            vmem(narrow, BF16),
            vmem((n, rows, 4 * side), BF16),
            vmem((n, rows, 4 * side), BF16),
            vmem((n, 1, 128), F32),
            vmem((n, 1, 128), F32),
            vmem((rows, 4 * side), F32),
            vmem((rows, side), F32),
            vmem((rows, side), BF16),
            vmem((n, rows, side), BF16),
            vmem(narrow, BF16),
            vmem(narrow, BF16),
            vmem((rows, cols), BF16),
            vmem(narrow, BF16),
            vmem((n, rows, 2 * up), BF16),
            vmem((n, rows, 2 * up), BF16),
            vmem((n, 1, 128), F32),
            vmem((n, 1, 128), F32),
            vmem((rows, 2 * up), F32),
            vmem((rows, up), BF16),
            vmem((n, rows, up), BF16),
            vmem(narrow, BF16),
            vmem(narrow, BF16),
            dma((8,)),
            dma,
            dma,
            dma((8,)),
            dma((8,)),
        ]
        + [dma((n,))] * 10,
        compiler_params=pltpu.CompilerParams(collective_id=0, has_side_effects=True),
        name="layer",
    )(
        tokens,
        state,
        mix_gain.reshape(1, -1),
        lower_bound.reshape(1, -1),
        head_gain.reshape(1, -1),
        ffn_gain.reshape(1, -1),
        q_weight,
        forget_weight,
        input_weight,
        gate_weight,
        out_weight,
        ffn_gate,
        ffn_up,
        ffn_down,
    )


def solution(mesh):
    in_specs = (
        P("tp", "kv"),
        P("kv", "tp", None, None),
        P("kv"),
        P("kv", "tp"),
        P("kv", "tp"),
        P("kv", "tp"),
        P("kv", "tp"),
        P("tp"),
        P(),
        P("tp", "kv"),
        P("kv"),
        P("kv", "tp"),
        P("kv", "tp"),
        P("tp", "kv"),
    )
    out_specs = (P("tp", "kv"), P("kv", "tp", None, None))
    return jax.shard_map(body, mesh=mesh, in_specs=in_specs, out_specs=out_specs, check_vma=False)
```

time: 180 us -> 120 us (0.67)
  blocking collectives: 129 us -> 0 us
  Pallas kernels: 0 us -> 111 us
  waiting for transfers between devices: 25.6 us -> 0 us
  other arithmetic: 10.3 us -> 0 us
  starting transfers between devices: 6.76 us -> 0 us
  local copies, waits for them, and re-layouts: 2.98 us -> 6.82 us
  matrix products: 3.68 us -> 0 us
    all_to_all x7 -> x0, blocking collectives: 129 us -> none  [the longest x4 66 us: from_everyone(): return lax.all_to_all(copies, axis, split_axis=0, concat_axis=0, tiled=True)]
    pallas_call x0 -> x1, Pallas kernels: none -> 111 us  [body(): pl.pallas_call(functools.partial(layer, n, nx, nz, cols * n), out_shape=(...]
    all_to_all x1 -> x0, waiting for transfers between devices: 25.6 us -> none  [sent_and_summed(): lax.all_to_all(cut_along(x.astype(jnp.bfloat16), dim, size), axis, 0, 0,...]
    all_to_all x1 -> x0, starting transfers between devices: 6.76 us -> none  [sent_and_summed(): lax.all_to_all(cut_along(x.astype(jnp.bfloat16), dim, size), axis, 0, 0,...]
    add x2 -> x0, other arithmetic: 6.59 us -> none  [the longest x1 6.56 us: body(): forget[..., None] * state + (1.0 - forget)[..., None] * value[:, :, None, :]]
    unnamed x18 -> x2, local copies, waits for them, and re-layouts: 1.58 us -> 6.82 us
    dot_general x5 -> x0, matrix products: 3.68 us -> none  [the longest x2 2.23 us: project_in(): product = jnp.dot(normed, weight_joined, preferred_element_type=jnp.float32)]
  transfers between devices with their start and end apart: 1 -> 0, of which waited for: 1 -> 0; matrix products, arithmetic and copies ran while one was open for 0% -> 0% of each run, Pallas kernels for 0% -> 0%
where the time goes in v2:
time: 120 us; the launch traced here: 119 us
  Pallas kernels  111 us (92%)
  local copies, waits for them, and re-layouts  6.82 us (6%)
    pallas_call x1, Pallas kernels, body(): pl.pallas_call(functools.partial(layer, n, nx, nz, cols * n), out_shape=(...  111 us
    unnamed x2, local copies, waits for them, and re-layouts  6.82 us

profile of v2, /device:TPU:1, one launch (start us, length us, event | category | flops | bytes accessed | tf_op | source)
XLA Modules:
  0.0 119.0 jit_solution(4434551609683711707)
XLA Ops:
  0.6 111.5 %layer.1 = (bf16[40,256]{1,0:T(8,128)(2,1)}, f32[40,2,128,128]{3,2,1,0:T(8,128)}) custom-call(bf16[40,256]{1,0:T(8,128)(2,1)} %tokens.1, f32[40,2,128,128]{3,2,1,0:T(8,128)} %state_in.1, f32[1,256]{1,0:T(1,128)} %bitcast.4, f32[1,256]{1,0:T(1,128)} %bitcast.5, f32[1,128]{1,0:T(1,128)} %bitcast.7, f32[1,256]{1,0:T(1,128)} %bitcast.6, bf16[256,256]{1,0:T(8,128)(2,1)} %wq_in.1, ...), custom_call_target="tpu_custom_call" | custom-call | tf_op jit(solution)/shard_map/layer/pallas_call | solution.py:332
  112.1 1.3 %copy.18 = bf16[40,256]{1,0:T(8,128)(2,1)} copy(bf16[40,256]{1,0:T(8,128)(2,1)} %get-tuple-element.4) | data formatting | bytes 40960
  113.5 5.5 %copy.19 = f32[40,2,128,128]{3,2,1,0:T(8,128)} copy(f32[40,2,128,128]{3,2,1,0:T(8,128)} %get-tuple-element.5) | data formatting | bytes 10485760

commit v3 on v1

v3 whole, which is shorter than its diff:
```python
import functools

import jax
import jax.numpy as jnp
from jax import lax
from jax.experimental import pallas as pl
from jax.experimental.pallas import tpu as pltpu
from jax.sharding import PartitionSpec as P

EPS = 1e-05
MESH = pl.DeviceIdType.MESH
F32 = jnp.float32
BF16 = jnp.bfloat16
HEAD = 128
EARLY = False


def ffn_chunks(up):
    first = (up // 256 + 1) * 128
    return ((0, first), (first, up - first))


def layer(n, nx, nz, width, *refs):
    (
        tokens,
        state_in,
        mix_gain,
        lower_bound,
        head_gain,
        ffn_gain,
        wq_in,
        wf_in,
        wi_in,
        wg_in,
        wo_in,
        wfg_in,
        wfu_in,
        wfd_in,
        out,
        forget_out,
        value_out,
        w_mix,
        w_out,
        w_ffn,
        w_down,
        state,
        x1,
        s2a,
        s2b,
        r2a,
        r2b,
        sq_s2,
        sq_r2,
        acc2,
        total,
        gated,
        g3,
        o4,
        p4,
        m4,
        s4,
        r4,
        own,
        x5,
        s6a,
        s6b,
        r6a,
        r6b,
        sq_s6,
        sq_r6,
        acc6a,
        acc6b,
        hida,
        hidb,
        h7a,
        h7b,
        o8,
        p8,
        m8,
        s8,
        r8,
        w_sem,
        st_sem,
        send_sem,
        x1_sem,
        r2a_sem,
        r2b_sem,
        q2_sem,
        g3_sem,
        p4_sem,
        r4_sem,
        x5_sem,
        r6a_sem,
        r6b_sem,
        q6_sem,
        h7a_sem,
        h7b_sem,
        p8_sem,
        r8_sem,
    ) = refs
    kv = lax.axis_index("kv")
    tp = lax.axis_index("tp")
    z, core = tp // 2, tp % 2
    mate = z * 2 + 1 - core
    ny = n // nx
    rows, cols = tokens.shape
    side = wq_in.shape[1]
    up = wfg_in.shape[1]
    heads = side // HEAD
    drains = []

    def kv_peer(j):
        x = (kv % nx + nx // 2 + nx - j % nx) % nx
        y = (kv // nx + ny // 2 + ny - j // nx) % ny
        return y * nx + x

    def kv_source(j):
        x = (kv % nx + nx // 2 + j % nx) % nx
        y = (kv // nx + ny // 2 + j // nx) % ny
        return y * nx + x

    def z_near(i):
        return (z + nz + jnp.where(i % 2 == 1, (i + 1) // 2, -(i // 2))) % nz

    def z_far(i):
        return z_near(nz - 1 - i)

    def loop(count, body):
        lax.fori_loop(0, count, lambda j, c: (body(j), c)[1], 0)

    barrier = pltpu.get_barrier_semaphore()

    def greet(who):
        pl.semaphore_signal(barrier, inc=1, device_id=who, device_id_type=MESH)

    @functools.partial(loop, n)
    def _(j):
        peer = kv_peer(j)

        @pl.when(peer != kv)
        def _():
            greet((peer, tp))

    @functools.partial(loop, nz - 1)
    def _(i):
        greet((kv, z_far(i) * 2 + core))

    greet((kv, mate))

    loads = []
    for h in range(heads):
        for k, w in enumerate((wq_in, wf_in, wi_in, wg_in)):
            loads.append(
                (w.at[:, pl.ds(h * HEAD, HEAD)], w_mix.at[:, pl.ds((4 * h + k) * HEAD, HEAD)])
            )
    n_mix = len(loads)
    loads.append((wo_in, w_out))
    for first, size in ffn_chunks(up):
        loads.append((wfg_in.at[:, pl.ds(first, size)], w_ffn.at[:, pl.ds(2 * first, size)]))
        loads.append((wfu_in.at[:, pl.ds(first, size)], w_ffn.at[:, pl.ds(2 * first + size, size)]))
    loads.append((wfd_in, w_down))
    loads = [pltpu.make_async_copy(a, b, w_sem.at[i]) for i, (a, b) in enumerate(loads)]
    for copy in loads:
        copy.start()
    state_load = pltpu.make_async_copy(state_in, state, st_sem)
    state_load.start()

    pl.semaphore_wait(barrier, (n - 1) + (nz - 1) + 1)

    def push(source, target, where, sent, landed, device):
        pltpu.make_async_remote_copy(
            src_ref=source,
            dst_ref=target.at[where],
            send_sem=sent,
            recv_sem=landed.at[where],
            device_id=device,
            device_id_type=MESH,
        ).start()

    def arrived(target, landed, who):
        pltpu.make_async_copy(target.at[who], target.at[who], landed.at[who]).wait()

    def to_kv(source, target, sent, landed, peer):
        @pl.when(peer != kv)
        def _():
            push(source, target, kv, sent, landed, (peer, tp))

        @pl.when(peer == kv)
        def _():
            pltpu.make_async_copy(source, target.at[kv], landed.at[kv]).start()

    def gather_kv(source, target, slot, landed):
        loop(n, lambda j: to_kv(source, target, send_sem.at[slot], landed, kv_peer(j)))
        drains.append((target, n - 1, slot))

    def gather_tp(source, target, slot, landed):
        target[tp] = source[...]
        sent = send_sem.at[slot]
        loop(
            nz - 1, lambda i: push(source, target, tp, sent, landed, (kv, z_far(i) * 2 + core))
        )
        push(source, target, tp, sent, landed, (kv, mate))
        drains.append((target, n - 1, slot))

    def projected(x, x_sem, x_slot, gain, weight, parts, sq_s, sq_r, q_sem, q_slot):
        ones = jnp.ones((8, cols), F32)
        sq_s[...] = jnp.zeros_like(sq_s)

        def step(i):
            @pl.when(i < nz)
            def _():
                here = z_near(i) * 2 + core

                @pl.when(i > 0)
                def _():
                    arrived(x, x_sem, here)
                    push(x.at[here], x, here, send_sem.at[x_slot], x_sem, (kv, mate))

            @pl.when(i > 0)
            def _():
                chip = z_near(i - 1)
                arrived(x, x_sem, chip * 2 + 1 - core)
                pair = pl.ds(chip * 2, 2)
                values = x[pair].reshape(2 * rows, cols).astype(F32)
                normed = (values * gain[...]).astype(BF16)
                for s, _, _, _, first, size in parts:
                    product = jnp.dot(
                        normed, weight[:, pl.ds(first, size)], preferred_element_type=F32
                    )
                    s[pair] = product.astype(BF16).reshape(2, rows, size)
                squares = lax.dot_general(
                    ones,
                    values * values,
                    (((1,), (1,)), ((), ())),
                    precision=lax.Precision.HIGHEST,
                    preferred_element_type=F32,
                )
                for k in range(2):
                    sq_s[chip * 2 + k, :, pl.ds(0, rows)] = squares[0:1, k * rows : (k + 1) * rows]
                if EARLY:
                    s, r, landed, slot, _, _ = parts[0]
                    for k in range(2):
                        peer = chip * 2 + (kv + k) % 2
                        to_kv(s.at[peer], r, send_sem.at[slot], landed, peer)

        loop(nz + 1, step)
        for p, (s, r, landed, slot, _, _) in enumerate(parts):

            def send(j):
                peer = kv_peer(j)
                if p > 0 or not EARLY:
                    to_kv(s.at[peer], r, send_sem.at[slot], landed, peer)
                if p == 0:
                    to_kv(sq_s.at[peer], sq_r, send_sem.at[q_slot], q_sem, peer)

            loop(n, send)
            drains.append((r, n - 1, slot))
        drains.append((sq_r, n - 1, q_slot))

    def add_up(count, source_of, target, landed, into):
        into[...] = jnp.zeros_like(into)

        def step(j):
            who = source_of(j)
            arrived(target, landed, who)
            into[...] += target[who].astype(F32)

        loop(count, step)

    def factor(sq_r, q_sem):
        def step(j, sums):
            who = kv_source(j)
            arrived(sq_r, q_sem, who)
            return sums + sq_r[who]

        sums = lax.fori_loop(0, n, step, jnp.zeros((1, 128), F32))
        row = lax.rsqrt(sums * (1.0 / width) + EPS)
        return jnp.transpose(jnp.broadcast_to(row, (128, 128)))[0:rows]

    def back(gs, weight, o, p, p_sem, p_slot, m, s, r, r_sem, r_slot):
        def step(i):
            @pl.when(i < nz)
            def _():
                chip = z_far(i)
                pair = pl.ds(chip * 2, 2)
                product = None
                for g, landed, first in gs:
                    arrived(g, landed, chip * 2)
                    arrived(g, landed, chip * 2 + 1)
                    size = g.shape[2]
                    term = jnp.dot(
                        g[pair].reshape(2 * rows, size),
                        weight[pl.ds(first, size), :],
                        preferred_element_type=F32,
                    )
                    product = term if product is None else product + term
                low, high = product[0:rows], product[rows : 2 * rows]
                o[chip] = jnp.where(core == 0, high, low).astype(BF16)
                push(o.at[chip], p, chip, send_sem.at[p_slot], p_sem, (kv, mate))
                m[chip] = jnp.where(core == 0, low, high)

            @pl.when(i > 0)
            def _():
                chip = z_far(i - 1)
                arrived(p, p_sem, chip)
                s[chip] = (m[chip] + p[chip].astype(F32)).astype(BF16)

                @pl.when(chip != z)
                def _():
                    push(s.at[chip], r, z, send_sem.at[r_slot], r_sem, (kv, chip * 2 + core))

                @pl.when(chip == z)
                def _():
                    pltpu.make_async_copy(s.at[chip], r.at[z], r_sem.at[z]).start()

        loop(nz + 1, step)
        drains.append((p, nz, p_slot))
        drains.append((r, nz - 1, r_slot))

    gather_tp(tokens, x1, 0, x1_sem)
    for copy in loads[0:n_mix]:
        copy.wait()
    parts = [
        (s2a, r2a, r2a_sem, 1, 0, 4 * HEAD),
        (s2b, r2b, r2b_sem, 2, 4 * HEAD, 4 * HEAD),
    ]
    projected(x1, x1_sem, 0, mix_gain, w_mix, parts, sq_s2, sq_r2, q2_sem, 3)

    scale = factor(sq_r2, q2_sem)
    state_load.wait()
    for h in range(heads):
        at = pl.ds(h * HEAD, HEAD)
        add_up(n, kv_source, (r2a, r2b)[h], (r2a_sem, r2b_sem)[h], acc2)
        query = acc2[:, 0:HEAD] * scale
        query = query * jax.nn.sigmoid(query) * (HEAD ** (-0.5))
        low = lower_bound[:, at]
        forget = low + (1.0 - low) * jax.nn.sigmoid(acc2[:, HEAD : 2 * HEAD] * scale)
        value = acc2[:, 2 * HEAD : 3 * HEAD] * scale
        gate = acc2[:, 3 * HEAD : 4 * HEAD] * scale
        forget_out[:, at] = forget
        value_out[:, at] = value
        kept = query * forget
        added = jnp.sum(query - kept, axis=-1, keepdims=True) * value
        acc2[:, 0:HEAD] = kept

        def eight(group, carry):
            eight_rows = pl.ds(pl.multiple_of(group * 8, 8), 8)
            columns = jnp.transpose(acc2[eight_rows, 0:HEAD])
            reads = []
            for b in range(8):
                reads.append(
                    jnp.sum(
                        columns[:, b : b + 1] * state[group * 8 + b, h], axis=0, keepdims=True
                    )
                )
            total[eight_rows, 0:HEAD] = jnp.concatenate(reads, axis=0)
            return carry

        lax.fori_loop(0, rows // 8, eight, 0)
        read = total[:, 0:HEAD] + added
        mean = jnp.mean(read * read, axis=-1, keepdims=True)
        read = read * lax.rsqrt(mean + EPS) * head_gain[...]
        gated[:, at] = (read * (gate * jax.nn.sigmoid(gate))).astype(BF16)

    gather_kv(gated, g3, 4, g3_sem)
    loads[n_mix].wait()
    back([(g3, g3_sem, 0)], w_out, o4, p4, p4_sem, 5, m4, s4, r4, r4_sem, 6)
    add_up(nz, z_near, r4, r4_sem, total)
    own[...] = (tokens[...].astype(F32) + total[...]).astype(BF16)

    gather_tp(own, x5, 7, x5_sem)
    for copy in loads[n_mix + 1 : -1]:
        copy.wait()
    (a_at, a_size), (b_at, b_size) = ffn_chunks(up)
    parts = [
        (s6a, r6a, r6a_sem, 8, 2 * a_at, 2 * a_size),
        (s6b, r6b, r6b_sem, 9, 2 * b_at, 2 * b_size),
    ]
    projected(x5, x5_sem, 7, ffn_gain, w_ffn, parts, sq_s6, sq_r6, q6_sem, 10)
    scale = factor(sq_r6, q6_sem)
    for r, landed, acc, hid, h7, h7_sem, slot in (
        (r6a, r6a_sem, acc6a, hida, h7a, h7a_sem, 11),
        (r6b, r6b_sem, acc6b, hidb, h7b, h7b_sem, 12),
    ):
        add_up(n, kv_source, r, landed, acc)
        size = hid.shape[1]
        for c in range(size // 128):
            gate = acc[:, c * 128 : (c + 1) * 128] * scale
            upper = acc[:, size + c * 128 : size + (c + 1) * 128] * scale
            hid[:, c * 128 : (c + 1) * 128] = (gate * jax.nn.sigmoid(gate) * upper).astype(BF16)
        gather_kv(hid, h7, slot, h7_sem)
    loads[-1].wait()
    gs = [(h7a, h7a_sem, a_at), (h7b, h7b_sem, b_at)]
    back(gs, w_down, o8, p8, p8_sem, 13, m8, s8, r8, r8_sem, 14)
    add_up(nz, z_near, r8, r8_sem, total)
    out[...] = (own[...].astype(F32) + total[...]).astype(BF16)

    for target, count, slot in drains:
        sent = target.at[pl.ds(0, count)]
        pltpu.make_async_copy(sent, sent, send_sem.at[slot]).wait()


def update(rows_in, forget, value, state, rows_out, state_out):
    rows_out[...] = rows_in[...]
    for h in range(state.shape[1]):
        columns = jnp.transpose(forget[:, h * HEAD : (h + 1) * HEAD])
        for b in range(8):
            v = value[b : b + 1, h * HEAD : (h + 1) * HEAD]
            state_out[b, h] = v + columns[:, b : b + 1] * (state[b, h] - v)


def body(
    tokens,
    state,
    mix_gain,
    q_weight,
    forget_weight,
    input_weight,
    gate_weight,
    lower_bound,
    head_gain,
    out_weight,
    ffn_gain,
    ffn_gate,
    ffn_up,
    ffn_down,
):
    n = lax.axis_size("kv")
    nx, nz = {16: (4, 8), 4: (2, 2)}[n]
    rows, cols = tokens.shape
    side, up = q_weight.shape[1], ffn_gate.shape[1]
    vmem, dma = pltpu.VMEM, pltpu.SemaphoreType.DMA
    in_vmem = pl.BlockSpec(memory_space=pltpu.VMEM)
    in_hbm = pl.BlockSpec(memory_space=pl.ANY)
    block = (rows, cols)
    all_blocks = vmem((n, *block), BF16)
    all_heads = vmem((n, rows, 4 * HEAD), BF16)
    chip_blocks = vmem((nz, *block), BF16)
    chip_sums = vmem((nz, *block), F32)
    squares = vmem((n, 1, 128), F32)
    (_, a_size), (_, b_size) = ffn_chunks(up)
    backward = [chip_blocks, chip_blocks, chip_sums, chip_blocks, chip_blocks]
    layer_out, forget, value = pl.pallas_call(
        functools.partial(layer, n, nx, nz, cols * n),
        out_shape=(
            jax.ShapeDtypeStruct(block, BF16),
            jax.ShapeDtypeStruct(block, F32),
            jax.ShapeDtypeStruct(block, F32),
        ),
        in_specs=[in_vmem, in_hbm, in_vmem, in_vmem, in_vmem, in_vmem] + [in_hbm] * 8,
        out_specs=(in_vmem, in_vmem, in_vmem),
        scratch_shapes=[
            vmem((cols, 4 * side), BF16),
            vmem(out_weight.shape, BF16),
            vmem((cols, 2 * up), BF16),
            vmem(ffn_down.shape, BF16),
            vmem(state.shape, F32),
            all_blocks,
            all_heads,
            all_heads,
            all_heads,
            all_heads,
            squares,
            squares,
            vmem((rows, 4 * HEAD), F32),
            vmem(block, F32),
            vmem(block, BF16),
            all_blocks,
            *backward,
            vmem(block, BF16),
            all_blocks,
            vmem((n, rows, 2 * a_size), BF16),
            vmem((n, rows, 2 * b_size), BF16),
            vmem((n, rows, 2 * a_size), BF16),
            vmem((n, rows, 2 * b_size), BF16),
            squares,
            squares,
            vmem((rows, 2 * a_size), F32),
            vmem((rows, 2 * b_size), F32),
            vmem((rows, a_size), BF16),
            vmem((rows, b_size), BF16),
            vmem((n, rows, a_size), BF16),
            vmem((n, rows, b_size), BF16),
            *backward,
            dma((4 * (side // HEAD) + 6,)),
            dma,
            dma((15,)),
            dma((n,)),
            dma((n,)),
            dma((n,)),
            dma((n,)),
            dma((n,)),
            dma((nz,)),
            dma((nz,)),
            dma((n,)),
            dma((n,)),
            dma((n,)),
            dma((n,)),
            dma((n,)),
            dma((n,)),
            dma((nz,)),
            dma((nz,)),
        ],
        compiler_params=pltpu.CompilerParams(collective_id=0, has_side_effects=True),
        name="layer",
    )(
        tokens,
        state,
        mix_gain.reshape(1, -1),
        lower_bound.reshape(1, -1),
        head_gain.reshape(1, -1),
        ffn_gain.reshape(1, -1),
        q_weight,
        forget_weight,
        input_weight,
        gate_weight,
        out_weight,
        ffn_gate,
        ffn_up,
        ffn_down,
    )
    eight = pl.BlockSpec((8, side), lambda i: (i, 0))
    states = pl.BlockSpec((8, *state.shape[1:]), lambda i: (i, 0, 0, 0))
    return pl.pallas_call(
        update,
        grid=(rows // 8,),
        out_shape=(
            jax.ShapeDtypeStruct(block, BF16),
            jax.ShapeDtypeStruct(state.shape, F32),
        ),
        in_specs=[pl.BlockSpec((8, cols), lambda i: (i, 0)), eight, eight, states],
        out_specs=(pl.BlockSpec((8, cols), lambda i: (i, 0)), states),
        name="update",
    )(layer_out, forget, value, state)


def solution(mesh):
    in_specs = (
        P("tp", "kv"),
        P("kv", "tp", None, None),
        P("kv"),
        P("kv", "tp"),
        P("kv", "tp"),
        P("kv", "tp"),
        P("kv", "tp"),
        P("tp"),
        P(),
        P("tp", "kv"),
        P("kv"),
        P("kv", "tp"),
        P("kv", "tp"),
        P("tp", "kv"),
    )
    out_specs = (P("tp", "kv"), P("kv", "tp", None, None))
    return jax.shard_map(body, mesh=mesh, in_specs=in_specs, out_specs=out_specs, check_vma=False)
```

time: 180 us -> 113 us (0.63)
  blocking collectives: 129 us -> 0 us
  Pallas kernels: 0 us -> 112 us
  waiting for transfers between devices: 25.6 us -> 0 us
  other arithmetic: 10.3 us -> 0 us
  starting transfers between devices: 6.76 us -> 0 us
  matrix products: 3.68 us -> 0 us
  local copies, waits for them, and re-layouts: 2.98 us -> 0 us
    all_to_all x7 -> x0, blocking collectives: 129 us -> none  [the longest x4 66 us: from_everyone(): return lax.all_to_all(copies, axis, split_axis=0, concat_axis=0, tiled=True)]
    pallas_call x0 -> x2, Pallas kernels: none -> 112 us  [the longest x1 104 us: body(): pl.pallas_call(functools.partial(layer, n, nx, nz, cols * n), out_shape=(...]
    all_to_all x1 -> x0, waiting for transfers between devices: 25.6 us -> none  [sent_and_summed(): lax.all_to_all(cut_along(x.astype(jnp.bfloat16), dim, size), axis, 0, 0,...]
    all_to_all x1 -> x0, starting transfers between devices: 6.76 us -> none  [sent_and_summed(): lax.all_to_all(cut_along(x.astype(jnp.bfloat16), dim, size), axis, 0, 0,...]
    add x2 -> x0, other arithmetic: 6.59 us -> none  [the longest x1 6.56 us: body(): forget[..., None] * state + (1.0 - forget)[..., None] * value[:, :, None, :]]
    dot_general x5 -> x0, matrix products: 3.68 us -> none  [the longest x2 2.23 us: project_in(): product = jnp.dot(normed, weight_joined, preferred_element_type=jnp.float32)]
  transfers between devices with their start and end apart: 1 -> 0, of which waited for: 1 -> 0; matrix products, arithmetic and copies ran while one was open for 0% -> 0% of each run, Pallas kernels for 0% -> 0%
where the time goes in v3:
time: 113 us
  Pallas kernels  112 us (99%)
    pallas_call x1, Pallas kernels, body(): pl.pallas_call(functools.partial(layer, n, nx, nz, cols * n), out_shape=(...  104 us
    pallas_call x1, Pallas kernels, body(): pl.pallas_call(update, grid=(rows // 8,), out_shape=(jax.ShapeDtypeStruct...  7.61 us

profile of v3, /device:TPU:1, one launch (start us, length us, event | category | flops | bytes accessed | tf_op | source)
XLA Modules:
  0.0 112.7 jit_solution(1822056223179237206)
XLA Ops:
  0.6 104.4 %layer.1 = (bf16[40,256]{1,0:T(8,128)(2,1)}, f32[40,256]{1,0:T(8,128)}, f32[40,256]{1,0:T(8,128)}) custom-call(bf16[40,256]{1,0:T(8,128)(2,1)} %refs_0_.1, f32[40,2,128,128]{3,2,1,0:T(8,128)} %state.1, f32[1,256]{1,0:T(1,128)} %bitcast.4, f32[1,256]{1,0:T(1,128)} %bitcast.5, f32[1,128]{1,0:T(1,128)} %bitcast.7, f32[1,256]{1,0:T(1,128)} %bitcast.6, ...), custom_call_target="tpu_custom_call" | custom-call | tf_op jit(solution)/shard_map/layer/pallas_call | solution.py:443
  105.1 7.6 %update.1 = (bf16[40,256]{1,0:T(8,128)(2,1)}, f32[40,2,128,128]{3,2,1,0:T(8,128)}) custom-call(bf16[40,256]{1,0:T(8,128)(2,1)} %get-tuple-element.5.rows_in, f32[40,256]{1,0:T(8,128)} %get-tuple-element.6.forget, f32[40,256]{1,0:T(8,128)} %get-tuple-element.7.value, f32[40,2,128,128]{3,2,1,0:T(8,128)} %state.1), custom_call_target="tpu_custom_call" | custom-call | tf_op jit(solution)/shard_map/update/pallas_call | solution.py:524

commit v4 on v3

--- a/solution.py
+++ b/solution.py
@@ -12,7 +12,6 @@
 F32 = jnp.float32
 BF16 = jnp.bfloat16
 HEAD = 128
-EARLY = False
 
 
 def ffn_chunks(up):
@@ -37,13 +36,13 @@
         wfu_in,
         wfd_in,
         out,
-        forget_out,
-        value_out,
+        state,
         w_mix,
         w_out,
         w_ffn,
         w_down,
-        state,
+        forgets,
+        values,
         x1,
         s2a,
         s2b,
@@ -54,7 +53,8 @@
         acc2,
         total,
         gated,
-        g3,
+        g3a,
+        g3b,
         o4,
         p4,
         m4,
@@ -86,7 +86,8 @@
         r2a_sem,
         r2b_sem,
         q2_sem,
-        g3_sem,
+        g3a_sem,
+        g3b_sem,
         p4_sem,
         r4_sem,
         x5_sem,
@@ -196,14 +197,16 @@
     def gather_tp(source, target, slot, landed):
         target[tp] = source[...]
         sent = send_sem.at[slot]
+        push(source, target, tp, sent, landed, (kv, mate))
         loop(
-            nz - 1, lambda i: push(source, target, tp, sent, landed, (kv, z_far(i) * 2 + core))
+            nz - 1,
+            lambda i: push(source, target, tp, sent, landed, (kv, z_near(i + 1) * 2 + core)),
         )
-        push(source, target, tp, sent, landed, (kv, mate))
         drains.append((target, n - 1, slot))
 
     def projected(x, x_sem, x_slot, gain, weight, parts, sq_s, sq_r, q_sem, q_slot):
         ones = jnp.ones((8, cols), F32)
+        lag = min(2, nz)
         sq_s[...] = jnp.zeros_like(sq_s)
 
         def step(i):
@@ -216,9 +219,9 @@
                     arrived(x, x_sem, here)
                     push(x.at[here], x, here, send_sem.at[x_slot], x_sem, (kv, mate))
 
-            @pl.when(i > 0)
+            @pl.when(i >= lag)
             def _():
-                chip = z_near(i - 1)
+                chip = z_near(i - lag)
                 arrived(x, x_sem, chip * 2 + 1 - core)
                 pair = pl.ds(chip * 2, 2)
                 values = x[pair].reshape(2 * rows, cols).astype(F32)
@@ -237,19 +240,13 @@
                 )
                 for k in range(2):
                     sq_s[chip * 2 + k, :, pl.ds(0, rows)] = squares[0:1, k * rows : (k + 1) * rows]
-                if EARLY:
-                    s, r, landed, slot, _, _ = parts[0]
-                    for k in range(2):
-                        peer = chip * 2 + (kv + k) % 2
-                        to_kv(s.at[peer], r, send_sem.at[slot], landed, peer)
-
-        loop(nz + 1, step)
+
+        loop(nz + lag, step)
         for p, (s, r, landed, slot, _, _) in enumerate(parts):
 
             def send(j):
                 peer = kv_peer(j)
-                if p > 0 or not EARLY:
-                    to_kv(s.at[peer], r, send_sem.at[slot], landed, peer)
+                to_kv(s.at[peer], r, send_sem.at[slot], landed, peer)
                 if p == 0:
                     to_kv(sq_s.at[peer], sq_r, send_sem.at[q_slot], q_sem, peer)
 
@@ -278,42 +275,40 @@
         return jnp.transpose(jnp.broadcast_to(row, (128, 128)))[0:rows]
 
     def back(gs, weight, o, p, p_sem, p_slot, m, s, r, r_sem, r_slot):
-        def step(i):
-            @pl.when(i < nz)
+        def multiply(i):
+            chip = z_far(i)
+            pair = pl.ds(chip * 2, 2)
+            product = None
+            for g, landed, first in gs:
+                arrived(g, landed, chip * 2)
+                arrived(g, landed, chip * 2 + 1)
+                size = g.shape[2]
+                term = jnp.dot(
+                    g[pair].reshape(2 * rows, size),
+                    weight[pl.ds(first, size), :],
+                    preferred_element_type=F32,
+                )
+                product = term if product is None else product + term
+            low, high = product[0:rows], product[rows : 2 * rows]
+            o[chip] = jnp.where(core == 0, high, low).astype(BF16)
+            push(o.at[chip], p, chip, send_sem.at[p_slot], p_sem, (kv, mate))
+            m[chip] = jnp.where(core == 0, low, high)
+
+        def pass_on(i):
+            chip = z_far(i)
+            arrived(p, p_sem, chip)
+            s[chip] = (m[chip] + p[chip].astype(F32)).astype(BF16)
+
+            @pl.when(chip != z)
             def _():
-                chip = z_far(i)
-                pair = pl.ds(chip * 2, 2)
-                product = None
-                for g, landed, first in gs:
-                    arrived(g, landed, chip * 2)
-                    arrived(g, landed, chip * 2 + 1)
-                    size = g.shape[2]
-                    term = jnp.dot(
-                        g[pair].reshape(2 * rows, size),
-                        weight[pl.ds(first, size), :],
-                        preferred_element_type=F32,
-                    )
-                    product = term if product is None else product + term
-                low, high = product[0:rows], product[rows : 2 * rows]
-                o[chip] = jnp.where(core == 0, high, low).astype(BF16)
-                push(o.at[chip], p, chip, send_sem.at[p_slot], p_sem, (kv, mate))
-                m[chip] = jnp.where(core == 0, low, high)
-
-            @pl.when(i > 0)
+                push(s.at[chip], r, z, send_sem.at[r_slot], r_sem, (kv, chip * 2 + core))
+
+            @pl.when(chip == z)
             def _():
-                chip = z_far(i - 1)
-                arrived(p, p_sem, chip)
-                s[chip] = (m[chip] + p[chip].astype(F32)).astype(BF16)
-
-                @pl.when(chip != z)
-                def _():
-                    push(s.at[chip], r, z, send_sem.at[r_slot], r_sem, (kv, chip * 2 + core))
-
-                @pl.when(chip == z)
-                def _():
-                    pltpu.make_async_copy(s.at[chip], r.at[z], r_sem.at[z]).start()
-
-        loop(nz + 1, step)
+                pltpu.make_async_copy(s.at[chip], r.at[z], r_sem.at[z]).start()
+
+        loop(nz, multiply)
+        loop(nz, pass_on)
         drains.append((p, nz, p_slot))
         drains.append((r, nz - 1, r_slot))
 
@@ -337,8 +332,8 @@
         forget = low + (1.0 - low) * jax.nn.sigmoid(acc2[:, HEAD : 2 * HEAD] * scale)
         value = acc2[:, 2 * HEAD : 3 * HEAD] * scale
         gate = acc2[:, 3 * HEAD : 4 * HEAD] * scale
-        forget_out[:, at] = forget
-        value_out[:, at] = value
+        forgets[:, at] = forget
+        values[:, at] = value
         kept = query * forget
         added = jnp.sum(query - kept, axis=-1, keepdims=True) * value
         acc2[:, 0:HEAD] = kept
@@ -360,11 +355,11 @@
         read = total[:, 0:HEAD] + added
         mean = jnp.mean(read * read, axis=-1, keepdims=True)
         read = read * lax.rsqrt(mean + EPS) * head_gain[...]
-        gated[:, at] = (read * (gate * jax.nn.sigmoid(gate))).astype(BF16)
-
-    gather_kv(gated, g3, 4, g3_sem)
+        gated[h] = (read * (gate * jax.nn.sigmoid(gate))).astype(BF16)
+        gather_kv(gated.at[h], (g3a, g3b)[h], (4, 15)[h], (g3a_sem, g3b_sem)[h])
+
     loads[n_mix].wait()
-    back([(g3, g3_sem, 0)], w_out, o4, p4, p4_sem, 5, m4, s4, r4, r4_sem, 6)
+    back([(g3a, g3a_sem, 0), (g3b, g3b_sem, HEAD)], w_out, o4, p4, p4_sem, 5, m4, s4, r4, r4_sem, 6)
     add_up(nz, z_near, r4, r4_sem, total)
     own[...] = (tokens[...].astype(F32) + total[...]).astype(BF16)
 
@@ -377,6 +372,19 @@
         (s6b, r6b, r6b_sem, 9, 2 * b_at, 2 * b_size),
     ]
     projected(x5, x5_sem, 7, ffn_gain, w_ffn, parts, sq_s6, sq_r6, q6_sem, 10)
+
+    def renew(group, carry):
+        first = pl.multiple_of(group * 8, 8)
+        for h in range(heads):
+            at = pl.ds(h * HEAD, HEAD)
+            columns = jnp.transpose(forgets[pl.ds(first, 8), at])
+            value = values[pl.ds(first, 8), at]
+            for b in range(8):
+                v = value[b : b + 1]
+                state[first + b, h] = v + columns[:, b : b + 1] * (state[first + b, h] - v)
+        return carry
+
+    lax.fori_loop(0, rows // 8, renew, 0)
     scale = factor(sq_r6, q6_sem)
     for r, landed, acc, hid, h7, h7_sem, slot in (
         (r6a, r6a_sem, acc6a, hida, h7a, h7a_sem, 11),
@@ -400,13 +408,15 @@
         pltpu.make_async_copy(sent, sent, send_sem.at[slot]).wait()
 
 
-def update(rows_in, forget, value, state, rows_out, state_out):
+def publish(rows_in, state_in, rows_out, state_out, sem):
+    copies = []
+    for i in range(state_in.shape[0] // 4):
+        at = pl.ds(i * 4, 4)
+        copies.append(pltpu.make_async_copy(state_in.at[at], state_out.at[at], sem.at[i]))
+        copies[-1].start()
     rows_out[...] = rows_in[...]
-    for h in range(state.shape[1]):
-        columns = jnp.transpose(forget[:, h * HEAD : (h + 1) * HEAD])
-        for b in range(8):
-            v = value[b : b + 1, h * HEAD : (h + 1) * HEAD]
-            state_out[b, h] = v + columns[:, b : b + 1] * (state[b, h] - v)
+    for copy in copies:
+        copy.wait()
 
 
 def body(
@@ -431,7 +441,7 @@
     side, up = q_weight.shape[1], ffn_gate.shape[1]
     vmem, dma = pltpu.VMEM, pltpu.SemaphoreType.DMA
     in_vmem = pl.BlockSpec(memory_space=pltpu.VMEM)
-    in_hbm = pl.BlockSpec(memory_space=pl.ANY)
+    in_hbm = pl.BlockSpec(memory_space=pltpu.HBM)
     block = (rows, cols)
     all_blocks = vmem((n, *block), BF16)
     all_heads = vmem((n, rows, 4 * HEAD), BF16)
@@ -440,21 +450,21 @@
     squares = vmem((n, 1, 128), F32)
     (_, a_size), (_, b_size) = ffn_chunks(up)
     backward = [chip_blocks, chip_blocks, chip_sums, chip_blocks, chip_blocks]
-    layer_out, forget, value = pl.pallas_call(
+    layer_out, new_state = pl.pallas_call(
         functools.partial(layer, n, nx, nz, cols * n),
         out_shape=(
-            jax.ShapeDtypeStruct(block, BF16),
-            jax.ShapeDtypeStruct(block, F32),
-            jax.ShapeDtypeStruct(block, F32),
+            pltpu.VMEM(block, BF16),
+            pltpu.VMEM(state.shape, F32),
         ),
         in_specs=[in_vmem, in_hbm, in_vmem, in_vmem, in_vmem, in_vmem] + [in_hbm] * 8,
-        out_specs=(in_vmem, in_vmem, in_vmem),
+        out_specs=(in_vmem, in_vmem),
         scratch_shapes=[
             vmem((cols, 4 * side), BF16),
             vmem(out_weight.shape, BF16),
             vmem((cols, 2 * up), BF16),
             vmem(ffn_down.shape, BF16),
-            vmem(state.shape, F32),
+            vmem(block, F32),
+            vmem(block, F32),
             all_blocks,
             all_heads,
             all_heads,
@@ -464,8 +474,9 @@
             squares,
             vmem((rows, 4 * HEAD), F32),
             vmem(block, F32),
-            vmem(block, BF16),
-            all_blocks,
+            vmem((side // HEAD, rows, HEAD), BF16),
+            vmem((n, rows, HEAD), BF16),
+            vmem((n, rows, HEAD), BF16),
             *backward,
             vmem(block, BF16),
             all_blocks,
@@ -484,7 +495,8 @@
             *backward,
             dma((4 * (side // HEAD) + 6,)),
             dma,
-            dma((15,)),
+            dma((16,)),
+            dma((n,)),
             dma((n,)),
             dma((n,)),
             dma((n,)),
@@ -501,7 +513,9 @@
             dma((nz,)),
             dma((nz,)),
         ],
-        compiler_params=pltpu.CompilerParams(collective_id=0, has_side_effects=True),
+        compiler_params=pltpu.CompilerParams(
+            collective_id=0, has_side_effects=True, vmem_limit_bytes=57 * 2**20
+        ),
         name="layer",
     )(
         tokens,
@@ -519,19 +533,18 @@
         ffn_up,
         ffn_down,
     )
-    eight = pl.BlockSpec((8, side), lambda i: (i, 0))
-    states = pl.BlockSpec((8, *state.shape[1:]), lambda i: (i, 0, 0, 0))
     return pl.pallas_call(
-        update,
-        grid=(rows // 8,),
+        publish,
         out_shape=(
             jax.ShapeDtypeStruct(block, BF16),
             jax.ShapeDtypeStruct(state.shape, F32),
         ),
-        in_specs=[pl.BlockSpec((8, cols), lambda i: (i, 0)), eight, eight, states],
-        out_specs=(pl.BlockSpec((8, cols), lambda i: (i, 0)), states),
-        name="update",
-    )(layer_out, forget, value, state)
+        in_specs=[in_vmem, in_vmem],
+        out_specs=(in_vmem, in_hbm),
+        scratch_shapes=[dma((rows // 4,))],
+        compiler_params=pltpu.CompilerParams(vmem_limit_bytes=8 * 2**20),
+        name="publish",
+    )(layer_out, new_state)
 
 
 def solution(mesh):

time: 113 us -> 106 us (0.938)
  Pallas kernels: 112 us -> 105 us
    pallas_call x1, Pallas kernels: 7.61 us -> 3.02 us  [body(): pl.pallas_call(publish, out_shape=(jax.ShapeDtypeStruct(block, BF16), jax...]
    pallas_call x1, Pallas kernels: 104 us -> 102 us  [body(): pl.pallas_call(functools.partial(layer, n, nx, nz, cols * n), out_shape=(...]
where the time goes in v4:
time: 106 us; the launch traced here: 105 us
  Pallas kernels  105 us (99%)
    pallas_call x1, Pallas kernels, body(): pl.pallas_call(functools.partial(layer, n, nx, nz, cols * n), out_shape=(...  102 us
    pallas_call x1, Pallas kernels, body(): pl.pallas_call(publish, out_shape=(jax.ShapeDtypeStruct(block, BF16), jax...  3.02 us

profile of v4, /device:TPU:1, one launch (start us, length us, event | category | flops | bytes accessed | tf_op | source)
XLA Modules:
  0.0 105.4 jit_solution(9946187968591195138)
XLA Ops:
  0.6 101.7 %layer.1 = (bf16[40,256]{1,0:T(8,128)(2,1)S(1)}, f32[40,2,128,128]{3,2,1,0:T(8,128)S(1)}) custom-call(bf16[40,256]{1,0:T(8,128)(2,1)} %refs_0_.1, f32[40,2,128,128]{3,2,1,0:T(8,128)} %refs_1_.1, f32[1,256]{1,0:T(1,128)} %bitcast.4, f32[1,256]{1,0:T(1,128)} %bitcast.5, f32[1,128]{1,0:T(1,128)} %bitcast.7, f32[1,256]{1,0:T(1,128)} %bitcast.6, ...), custom_call_target="tpu_custom_call" | custom-call | tf_op jit(solution)/shard_map/layer/pallas_call | solution.py:453
  102.4 3.0 %publish.1 = (bf16[40,256]{1,0:T(8,128)(2,1)}, f32[40,2,128,128]{3,2,1,0:T(8,128)}) custom-call(bf16[40,256]{1,0:T(8,128)(2,1)S(1)} %get-tuple-element.4.rows_in, f32[40,2,128,128]{3,2,1,0:T(8,128)S(1)} %get-tuple-element.5.state_in), custom_call_target="tpu_custom_call" | custom-call | tf_op jit(solution)/shard_map/publish/pallas_call | solution.py:536

commit v5 on v4

--- a/solution.py
+++ b/solution.py
@@ -14,9 +14,7 @@
 HEAD = 128
 
 
-def ffn_chunks(up):
-    first = (up // 256 + 1) * 128
-    return ((0, first), (first, up - first))
+WIDE = 2 * HEAD
 
 
 def layer(n, nx, nz, width, *refs):
@@ -44,10 +42,10 @@
         forgets,
         values,
         x1,
-        s2a,
-        s2b,
-        r2a,
-        r2b,
+        s2,
+        t2,
+        u2,
+        v2,
         sq_s2,
         sq_r2,
         acc2,
@@ -62,14 +60,14 @@
         r4,
         own,
         x5,
-        s6a,
-        s6b,
-        r6a,
-        r6b,
+        s6,
+        t6,
+        u6,
+        v6,
+        d6,
         sq_s6,
         sq_r6,
-        acc6a,
-        acc6b,
+        acc6,
         hida,
         hidb,
         h7a,
@@ -83,16 +81,17 @@
         st_sem,
         send_sem,
         x1_sem,
-        r2a_sem,
-        r2b_sem,
+        t2_sem,
+        v2_sem,
         q2_sem,
         g3a_sem,
         g3b_sem,
         p4_sem,
         r4_sem,
         x5_sem,
-        r6a_sem,
-        r6b_sem,
+        t6_sem,
+        v6_sem,
+        d6_sem,
         q6_sem,
         h7a_sem,
         h7b_sem,
@@ -156,9 +155,12 @@
             )
     n_mix = len(loads)
     loads.append((wo_in, w_out))
-    for first, size in ffn_chunks(up):
-        loads.append((wfg_in.at[:, pl.ds(first, size)], w_ffn.at[:, pl.ds(2 * first, size)]))
-        loads.append((wfu_in.at[:, pl.ds(first, size)], w_ffn.at[:, pl.ds(2 * first + size, size)]))
+    units = up // HEAD
+    for c in range(units):
+        for k, w in enumerate((wfg_in, wfu_in)):
+            loads.append(
+                (w.at[:, pl.ds(c * HEAD, HEAD)], w_ffn.at[:, pl.ds((2 * c + k) * HEAD, HEAD)])
+            )
     loads.append((wfd_in, w_down))
     loads = [pltpu.make_async_copy(a, b, w_sem.at[i]) for i, (a, b) in enumerate(loads)]
     for copy in loads:
@@ -204,7 +206,7 @@
         )
         drains.append((target, n - 1, slot))
 
-    def projected(x, x_sem, x_slot, gain, weight, parts, sq_s, sq_r, q_sem, q_slot):
+    def projected(x, x_sem, x_slot, gain, weight, s, orders, sq_s, sq_r, q_sem, q_slot):
         ones = jnp.ones((8, cols), F32)
         lag = min(2, nz)
         sq_s[...] = jnp.zeros_like(sq_s)
@@ -223,14 +225,17 @@
             def _():
                 chip = z_near(i - lag)
                 arrived(x, x_sem, chip * 2 + 1 - core)
-                pair = pl.ds(chip * 2, 2)
-                values = x[pair].reshape(2 * rows, cols).astype(F32)
+                values = x[pl.ds(chip * 2, 2)].reshape(2 * rows, cols).astype(F32)
                 normed = (values * gain[...]).astype(BF16)
-                for s, _, _, _, first, size in parts:
+                for c, order in enumerate(orders):
                     product = jnp.dot(
-                        normed, weight[:, pl.ds(first, size)], preferred_element_type=F32
-                    )
-                    s[pair] = product.astype(BF16).reshape(2, rows, size)
+                        normed, weight[:, c * WIDE : (c + 1) * WIDE], preferred_element_type=F32
+                    ).astype(BF16)
+                    for k in range(2):
+                        at = chip * 2 + k
+                        if order == "x":
+                            at = (at % nx) * ny + at // nx
+                        s[c, at] = product[k * rows : (k + 1) * rows]
                 squares = lax.dot_general(
                     ones,
                     values * values,
@@ -242,17 +247,61 @@
                     sq_s[chip * 2 + k, :, pl.ds(0, rows)] = squares[0:1, k * rows : (k + 1) * rows]
 
         loop(nz + lag, step)
-        for p, (s, r, landed, slot, _, _) in enumerate(parts):
-
+
+        def send_squares():
             def send(j):
                 peer = kv_peer(j)
-                to_kv(s.at[peer], r, send_sem.at[slot], landed, peer)
-                if p == 0:
-                    to_kv(sq_s.at[peer], sq_r, send_sem.at[q_slot], q_sem, peer)
+                to_kv(sq_s.at[peer], sq_r, send_sem.at[q_slot], q_sem, peer)
 
             loop(n, send)
-            drains.append((r, n - 1, slot))
-        drains.append((sq_r, n - 1, q_slot))
+            drains.append((sq_r, n - 1, q_slot))
+
+        return send_squares
+
+    rings = {
+        "x": (kv % nx, nx, lambda p: (kv // nx * nx + p, tp)),
+        "y": (kv // nx, ny, lambda p: (p * nx + kv % nx, tp)),
+    }
+
+    def around(axis):
+        me, size, _ = rings[axis]
+        far_first = sorted(range(1, size), key=lambda d: -min(d, size - d))
+        return [(me + d) % size for d in far_first]
+
+    def two_stages(order, c, s, t, u, v, t_sem, v_sem, slot):
+        first, second = order, "y" if order == "x" else "x"
+        me, size, place = rings[first]
+        then, others, then_place = rings[second]
+        s, t, u, v = s.at[c], t.at[c], u.at[c], v.at[c]
+        t_sem, v_sem = t_sem.at[c], v_sem.at[c]
+
+        def start():
+            for p in around(first):
+                block = s.at[pl.ds(p * others, others)]
+                push(block, t, me, send_sem.at[slot], t_sem, place(p))
+            drains.append((t, size - 1, slot))
+
+        def middle():
+            for p in around(first):
+                arrived(t, t_sem, p)
+            for q in around(second) + [then]:
+                sums = s[me * others + q].astype(F32)
+                for p in around(first):
+                    sums += t[p, q].astype(F32)
+                u[q] = sums.astype(BF16)
+                if q is not then:
+                    push(u.at[q], v, then, send_sem.at[slot + 1], v_sem, then_place(q))
+            drains.append((v, others - 1, slot + 1))
+
+        def finish():
+            for q in around(second):
+                arrived(v, v_sem, q)
+            sums = u[then].astype(F32)
+            for q in around(second):
+                sums += v[q].astype(F32)
+            return sums
+
+        return start, middle, finish
 
     def add_up(count, source_of, target, landed, into):
         into[...] = jnp.zeros_like(into)
@@ -315,17 +364,26 @@
     gather_tp(tokens, x1, 0, x1_sem)
     for copy in loads[0:n_mix]:
         copy.wait()
-    parts = [
-        (s2a, r2a, r2a_sem, 1, 0, 4 * HEAD),
-        (s2b, r2b, r2b_sem, 2, 4 * HEAD, 4 * HEAD),
+    orders = ["x", "y"] * heads
+    send_squares = projected(
+        x1, x1_sem, 0, mix_gain, w_mix, s2, orders, sq_s2, sq_r2, q2_sem, 1
+    )
+    stages = [
+        two_stages(order, c, s2, t2, u2, v2, t2_sem, v2_sem, 2 + 2 * c)
+        for c, order in enumerate(orders)
     ]
-    projected(x1, x1_sem, 0, mix_gain, w_mix, parts, sq_s2, sq_r2, q2_sem, 3)
+    for start, _, _ in stages:
+        start()
+    send_squares()
+    for _, middle, _ in stages:
+        middle()
 
     scale = factor(sq_r2, q2_sem)
     state_load.wait()
     for h in range(heads):
         at = pl.ds(h * HEAD, HEAD)
-        add_up(n, kv_source, (r2a, r2b)[h], (r2a_sem, r2b_sem)[h], acc2)
+        acc2[:, 0:WIDE] = stages[2 * h][2]()
+        acc2[:, WIDE : 2 * WIDE] = stages[2 * h + 1][2]()
         query = acc2[:, 0:HEAD] * scale
         query = query * jax.nn.sigmoid(query) * (HEAD ** (-0.5))
         low = lower_bound[:, at]
@@ -356,22 +414,27 @@
         mean = jnp.mean(read * read, axis=-1, keepdims=True)
         read = read * lax.rsqrt(mean + EPS) * head_gain[...]
         gated[h] = (read * (gate * jax.nn.sigmoid(gate))).astype(BF16)
-        gather_kv(gated.at[h], (g3a, g3b)[h], (4, 15)[h], (g3a_sem, g3b_sem)[h])
+        gather_kv(gated.at[h], (g3a, g3b)[h], (10, 11)[h], (g3a_sem, g3b_sem)[h])
 
     loads[n_mix].wait()
-    back([(g3a, g3a_sem, 0), (g3b, g3b_sem, HEAD)], w_out, o4, p4, p4_sem, 5, m4, s4, r4, r4_sem, 6)
+    back([(g3a, g3a_sem, 0), (g3b, g3b_sem, HEAD)], w_out, o4, p4, p4_sem, 12, m4, s4, r4, r4_sem, 13)
     add_up(nz, z_near, r4, r4_sem, total)
     own[...] = (tokens[...].astype(F32) + total[...]).astype(BF16)
 
-    gather_tp(own, x5, 7, x5_sem)
+    gather_tp(own, x5, 14, x5_sem)
     for copy in loads[n_mix + 1 : -1]:
         copy.wait()
-    (a_at, a_size), (b_at, b_size) = ffn_chunks(up)
-    parts = [
-        (s6a, r6a, r6a_sem, 8, 2 * a_at, 2 * a_size),
-        (s6b, r6b, r6b_sem, 9, 2 * b_at, 2 * b_size),
+    orders = [("x", "y")[c % 2] for c in range(units - 1)] + ["direct"]
+    send_squares = projected(
+        x5, x5_sem, 14, ffn_gain, w_ffn, s6, orders, sq_s6, sq_r6, q6_sem, 15
+    )
+    stages = [
+        two_stages(order, c, s6, t6, u6, v6, t6_sem, v6_sem, 16 + 2 * c)
+        for c, order in enumerate(orders[:-1])
     ]
-    projected(x5, x5_sem, 7, ffn_gain, w_ffn, parts, sq_s6, sq_r6, q6_sem, 10)
+    for start, _, _ in stages:
+        start()
+    send_squares()
 
     def renew(group, carry):
         first = pl.multiple_of(group * 8, 8)
@@ -385,21 +448,31 @@
         return carry
 
     lax.fori_loop(0, rows // 8, renew, 0)
+    stages[0][1]()
+    stages[1][1]()
+    direct = s6.at[units - 1]
+    loop(n, lambda j: to_kv(direct.at[kv_peer(j)], d6, send_sem.at[24], d6_sem, kv_peer(j)))
+    drains.append((d6, n - 1, 24))
+    for _, middle, _ in stages[2:]:
+        middle()
     scale = factor(sq_r6, q6_sem)
-    for r, landed, acc, hid, h7, h7_sem, slot in (
-        (r6a, r6a_sem, acc6a, hida, h7a, h7a_sem, 11),
-        (r6b, r6b_sem, acc6b, hidb, h7b, h7b_sem, 12),
-    ):
-        add_up(n, kv_source, r, landed, acc)
-        size = hid.shape[1]
-        for c in range(size // 128):
-            gate = acc[:, c * 128 : (c + 1) * 128] * scale
-            upper = acc[:, size + c * 128 : size + (c + 1) * 128] * scale
-            hid[:, c * 128 : (c + 1) * 128] = (gate * jax.nn.sigmoid(gate) * upper).astype(BF16)
-        gather_kv(hid, h7, slot, h7_sem)
+
+    def activate(sums, hid, c):
+        gate, upper = sums[:, 0:HEAD] * scale, sums[:, HEAD:WIDE] * scale
+        hid[:, c * HEAD : (c + 1) * HEAD] = (gate * jax.nn.sigmoid(gate) * upper).astype(BF16)
+
+    early = 2
+    for c in range(early):
+        activate(stages[c][2](), hida, c)
+    gather_kv(hida, h7a, 25, h7a_sem)
+    for c in range(early, units - 1):
+        activate(stages[c][2](), hidb, c - early)
+    add_up(n, kv_source, d6, d6_sem, acc6)
+    activate(acc6[...], hidb, units - 1 - early)
+    gather_kv(hidb, h7b, 26, h7b_sem)
     loads[-1].wait()
-    gs = [(h7a, h7a_sem, a_at), (h7b, h7b_sem, b_at)]
-    back(gs, w_down, o8, p8, p8_sem, 13, m8, s8, r8, r8_sem, 14)
+    gs = [(h7a, h7a_sem, 0), (h7b, h7b_sem, early * HEAD)]
+    back(gs, w_down, o8, p8, p8_sem, 27, m8, s8, r8, r8_sem, 28)
     add_up(nz, z_near, r8, r8_sem, total)
     out[...] = (own[...].astype(F32) + total[...]).astype(BF16)
 
@@ -409,12 +482,12 @@
 
 
 def publish(rows_in, state_in, rows_out, state_out, sem):
-    copies = []
+    copies = [pltpu.make_async_copy(rows_in, rows_out, sem.at[0])]
     for i in range(state_in.shape[0] // 4):
         at = pl.ds(i * 4, 4)
-        copies.append(pltpu.make_async_copy(state_in.at[at], state_out.at[at], sem.at[i]))
-        copies[-1].start()
-    rows_out[...] = rows_in[...]
+        copies.append(pltpu.make_async_copy(state_in.at[at], state_out.at[at], sem.at[i + 1]))
+    for copy in copies:
+        copy.start()
     for copy in copies:
         copy.wait()
 
@@ -444,11 +517,19 @@
     in_hbm = pl.BlockSpec(memory_space=pltpu.HBM)
     block = (rows, cols)
     all_blocks = vmem((n, *block), BF16)
-    all_heads = vmem((n, rows, 4 * HEAD), BF16)
     chip_blocks = vmem((nz, *block), BF16)
     chip_sums = vmem((nz, *block), F32)
     squares = vmem((n, 1, 128), F32)
-    (_, a_size), (_, b_size) = ffn_chunks(up)
+    ny, wide = n // nx, 2 * HEAD
+    units, mixed = up // HEAD, 2 * (side // HEAD)
+
+    def staged(chunks):
+        return [
+            vmem((chunks, nx, ny, rows, wide), BF16),
+            vmem((chunks, nx, rows, wide), BF16),
+            vmem((chunks, nx, rows, wide), BF16),
+        ]
+
     backward = [chip_blocks, chip_blocks, chip_sums, chip_blocks, chip_blocks]
     layer_out, new_state = pl.pallas_call(
         functools.partial(layer, n, nx, nz, cols * n),
@@ -466,10 +547,8 @@
             vmem(block, F32),
             vmem(block, F32),
             all_blocks,
-            all_heads,
-            all_heads,
-            all_heads,
-            all_heads,
+            vmem((mixed, n, rows, wide), BF16),
+            *staged(mixed),
             squares,
             squares,
             vmem((rows, 4 * HEAD), F32),
@@ -480,32 +559,31 @@
             *backward,
             vmem(block, BF16),
             all_blocks,
-            vmem((n, rows, 2 * a_size), BF16),
-            vmem((n, rows, 2 * b_size), BF16),
-            vmem((n, rows, 2 * a_size), BF16),
-            vmem((n, rows, 2 * b_size), BF16),
+            vmem((units, n, rows, wide), BF16),
+            *staged(units - 1),
+            vmem((n, rows, wide), BF16),
             squares,
             squares,
-            vmem((rows, 2 * a_size), F32),
-            vmem((rows, 2 * b_size), F32),
-            vmem((rows, a_size), BF16),
-            vmem((rows, b_size), BF16),
-            vmem((n, rows, a_size), BF16),
-            vmem((n, rows, b_size), BF16),
+            vmem((rows, wide), F32),
+            vmem((rows, 2 * HEAD), BF16),
+            vmem((rows, up - 2 * HEAD), BF16),
+            vmem((n, rows, 2 * HEAD), BF16),
+            vmem((n, rows, up - 2 * HEAD), BF16),
             *backward,
-            dma((4 * (side // HEAD) + 6,)),
+            dma((2 * mixed + 2 * units + 2,)),
             dma,
-            dma((16,)),
-            dma((n,)),
-            dma((n,)),
-            dma((n,)),
+            dma((29,)),
+            dma((n,)),
+            dma((mixed, nx)),
+            dma((mixed, nx)),
             dma((n,)),
             dma((n,)),
             dma((n,)),
             dma((nz,)),
             dma((nz,)),
             dma((n,)),
-            dma((n,)),
+            dma((units - 1, nx)),
+            dma((units - 1, nx)),
             dma((n,)),
             dma((n,)),
             dma((n,)),
@@ -540,8 +618,8 @@
             jax.ShapeDtypeStruct(state.shape, F32),
         ),
         in_specs=[in_vmem, in_vmem],
-        out_specs=(in_vmem, in_hbm),
-        scratch_shapes=[dma((rows // 4,))],
+        out_specs=(in_hbm, in_hbm),
+        scratch_shapes=[dma((rows // 4 + 1,))],
         compiler_params=pltpu.CompilerParams(vmem_limit_bytes=8 * 2**20),
         name="publish",
     )(layer_out, new_state)

time: 106 us -> 92.7 us (0.87)
  Pallas kernels: 105 us -> 91.9 us
    pallas_call x1, Pallas kernels: 102 us -> 89.5 us  [body(): pl.pallas_call(functools.partial(layer, n, nx, nz, cols * n), out_shape=(...]
where the time goes in v5:
time: 92.7 us; the launch traced here: 92.6 us
  Pallas kernels  91.9 us (99%)
    pallas_call x1, Pallas kernels, body(): pl.pallas_call(functools.partial(layer, n, nx, nz, cols * n), out_shape=(...  89.5 us
    pallas_call x1, Pallas kernels, body(): pl.pallas_call(publish, out_shape=(jax.ShapeDtypeStruct(block, BF16), jax...  2.43 us

profile of v5, /device:TPU:1, one launch (start us, length us, event | category | flops | bytes accessed | tf_op | source)
XLA Modules:
  0.0 92.6 jit_solution(17744671875900597349)
XLA Ops:
  0.6 89.5 %layer.1 = (bf16[40,256]{1,0:T(8,128)(2,1)S(1)}, f32[40,2,128,128]{3,2,1,0:T(8,128)S(1)}) custom-call(bf16[40,256]{1,0:T(8,128)(2,1)} %refs_0_.1, f32[40,2,128,128]{3,2,1,0:T(8,128)} %refs_1_.1, f32[1,256]{1,0:T(1,128)} %bitcast.4, f32[1,256]{1,0:T(1,128)} %bitcast.5, f32[1,128]{1,0:T(1,128)} %bitcast.7, f32[1,256]{1,0:T(1,128)} %bitcast.6, ...), custom_call_target="tpu_custom_call" | custom-call | tf_op jit(solution)/shard_map/layer/pallas_call | solution.py:534
  90.1 2.4 %publish.1 = (bf16[40,256]{1,0:T(8,128)(2,1)}, f32[40,2,128,128]{3,2,1,0:T(8,128)}) custom-call(bf16[40,256]{1,0:T(8,128)(2,1)S(1)} %get-tuple-element.4.rows_in, f32[40,2,128,128]{3,2,1,0:T(8,128)S(1)} %get-tuple-element.5.state_in), custom_call_target="tpu_custom_call" | custom-call | tf_op jit(solution)/shard_map/publish/pallas_call | solution.py:614

commit v6 on v5

--- a/solution.py
+++ b/solution.py
@@ -19,12 +19,12 @@
 
 def layer(n, nx, nz, width, *refs):
     (
-        tokens,
+        tokens_in,
         state_in,
-        mix_gain,
-        lower_bound,
-        head_gain,
-        ffn_gain,
+        mix_gain_in,
+        lower_bound_in,
+        head_gain_in,
+        ffn_gain_in,
         wq_in,
         wf_in,
         wi_in,
@@ -34,7 +34,13 @@
         wfu_in,
         wfd_in,
         out,
+        state_out,
         state,
+        tokens,
+        mix_gain,
+        lower_bound,
+        head_gain,
+        ffn_gain,
         w_mix,
         w_out,
         w_ffn,
@@ -51,8 +57,7 @@
         acc2,
         total,
         gated,
-        g3a,
-        g3b,
+        g3,
         o4,
         p4,
         m4,
@@ -64,37 +69,41 @@
         t6,
         u6,
         v6,
-        d6,
+        s7,
+        t7,
+        u7,
+        v7,
         sq_s6,
         sq_r6,
-        acc6,
-        hida,
-        hidb,
-        h7a,
-        h7b,
+        hidden,
+        h7,
+        h7c,
         o8,
         p8,
         m8,
         s8,
         r8,
+        small_sem,
         w_sem,
         st_sem,
+        so_sem,
         send_sem,
         x1_sem,
         t2_sem,
         v2_sem,
         q2_sem,
-        g3a_sem,
-        g3b_sem,
+        g3_sem,
         p4_sem,
         r4_sem,
         x5_sem,
         t6_sem,
         v6_sem,
-        d6_sem,
+        t7_sem,
+        v7_sem,
         q6_sem,
-        h7a_sem,
-        h7b_sem,
+        h7_sem,
+        h7_line_sem,
+        h7c_sem,
         p8_sem,
         r8_sem,
     ) = refs
@@ -128,6 +137,16 @@
     def loop(count, body):
         lax.fori_loop(0, count, lambda j, c: (body(j), c)[1], 0)
 
+    smalls = (
+        (tokens_in, tokens),
+        (mix_gain_in, mix_gain),
+        (lower_bound_in, lower_bound),
+        (head_gain_in, head_gain),
+        (ffn_gain_in, ffn_gain),
+    )
+    smalls = [pltpu.make_async_copy(a, b, small_sem.at[i]) for i, (a, b) in enumerate(smalls)]
+    for copy in smalls:
+        copy.start()
     barrier = pltpu.get_barrier_semaphore()
 
     def greet(who):
@@ -162,23 +181,28 @@
                 (w.at[:, pl.ds(c * HEAD, HEAD)], w_ffn.at[:, pl.ds((2 * c + k) * HEAD, HEAD)])
             )
     loads.append((wfd_in, w_down))
-    loads = [pltpu.make_async_copy(a, b, w_sem.at[i]) for i, (a, b) in enumerate(loads)]
+    kinds = [0] * n_mix + [1] + [2] * (2 * units) + [3]
+    loads = [pltpu.make_async_copy(a, b, w_sem.at[k]) for k, (a, b) in zip(kinds, loads)]
     for copy in loads:
         copy.start()
     state_load = pltpu.make_async_copy(state_in, state, st_sem)
     state_load.start()
-
     pl.semaphore_wait(barrier, (n - 1) + (nz - 1) + 1)
+    for copy in smalls:
+        copy.wait()
 
     def push(source, target, where, sent, landed, device):
         pltpu.make_async_remote_copy(
             src_ref=source,
             dst_ref=target.at[where],
             send_sem=sent,
-            recv_sem=landed.at[where],
+            recv_sem=landed,
             device_id=device,
             device_id_type=MESH,
         ).start()
+
+    def all_of(ref, semaphore):
+        pltpu.make_async_copy(ref, ref, semaphore).wait()
 
     def arrived(target, landed, who):
         pltpu.make_async_copy(target.at[who], target.at[who], landed.at[who]).wait()
@@ -190,23 +214,24 @@
 
         @pl.when(peer == kv)
         def _():
-            pltpu.make_async_copy(source, target.at[kv], landed.at[kv]).start()
-
-    def gather_kv(source, target, slot, landed):
-        loop(n, lambda j: to_kv(source, target, send_sem.at[slot], landed, kv_peer(j)))
-        drains.append((target, n - 1, slot))
+            pltpu.make_async_copy(source, target.at[kv], landed).start()
+
+    def gather_kv(source, target, sent, landed):
+        loop(n, lambda j: to_kv(source, target, sent, landed, kv_peer(j)))
 
     def gather_tp(source, target, slot, landed):
         target[tp] = source[...]
         sent = send_sem.at[slot]
-        push(source, target, tp, sent, landed, (kv, mate))
+        push(source, target, tp, sent, landed.at[tp], (kv, mate))
         loop(
             nz - 1,
-            lambda i: push(source, target, tp, sent, landed, (kv, z_near(i + 1) * 2 + core)),
+            lambda i: push(
+                source, target, tp, sent, landed.at[tp], (kv, z_near(i + 1) * 2 + core)
+            ),
         )
-        drains.append((target, n - 1, slot))
-
-    def projected(x, x_sem, x_slot, gain, weight, s, orders, sq_s, sq_r, q_sem, q_slot):
+        drains.append((target.at[pl.ds(0, n - 1)], slot))
+
+    def projected(x, x_sem, x_slot, gain, weight, s, orders, halves, sq_s, sq_r, q_sem, q_slot):
         ones = jnp.ones((8, cols), F32)
         lag = min(2, nz)
         sq_s[...] = jnp.zeros_like(sq_s)
@@ -219,7 +244,7 @@
                 @pl.when(i > 0)
                 def _():
                     arrived(x, x_sem, here)
-                    push(x.at[here], x, here, send_sem.at[x_slot], x_sem, (kv, mate))
+                    push(x.at[here], x, here, send_sem.at[x_slot], x_sem.at[here], (kv, mate))
 
             @pl.when(i >= lag)
             def _():
@@ -232,10 +257,14 @@
                         normed, weight[:, c * WIDE : (c + 1) * WIDE], preferred_element_type=F32
                     ).astype(BF16)
                     for k in range(2):
-                        at = chip * 2 + k
-                        if order == "x":
-                            at = (at % nx) * ny + at // nx
-                        s[c, at] = product[k * rows : (k + 1) * rows]
+                        y_at = chip * 2 + k
+                        x_at = (y_at % nx) * ny + y_at // nx
+                        part = product[k * rows : (k + 1) * rows]
+                        if order == "both":
+                            halves[0, x_at] = part[:, 0:HEAD]
+                            halves[1, y_at] = part[:, HEAD:WIDE]
+                        else:
+                            s[c, x_at if order == "x" else y_at] = part
                 squares = lax.dot_general(
                     ones,
                     values * values,
@@ -254,7 +283,7 @@
                 to_kv(sq_s.at[peer], sq_r, send_sem.at[q_slot], q_sem, peer)
 
             loop(n, send)
-            drains.append((sq_r, n - 1, q_slot))
+            drains.append((sq_r.at[pl.ds(0, n - 1)], q_slot))
 
         return send_squares
 
@@ -279,11 +308,9 @@
             for p in around(first):
                 block = s.at[pl.ds(p * others, others)]
                 push(block, t, me, send_sem.at[slot], t_sem, place(p))
-            drains.append((t, size - 1, slot))
 
         def middle():
-            for p in around(first):
-                arrived(t, t_sem, p)
+            all_of(t.at[pl.ds(0, size - 1)], t_sem)
             for q in around(second) + [then]:
                 sums = s[me * others + q].astype(F32)
                 for p in around(first):
@@ -291,11 +318,9 @@
                 u[q] = sums.astype(BF16)
                 if q is not then:
                     push(u.at[q], v, then, send_sem.at[slot + 1], v_sem, then_place(q))
-            drains.append((v, others - 1, slot + 1))
 
         def finish():
-            for q in around(second):
-                arrived(v, v_sem, q)
+            all_of(v.at[pl.ds(0, others - 1)], v_sem)
             sums = u[then].astype(F32)
             for q in around(second):
                 sums += v[q].astype(F32)
@@ -303,44 +328,66 @@
 
         return start, middle, finish
 
-    def add_up(count, source_of, target, landed, into):
-        into[...] = jnp.zeros_like(into)
-
-        def step(j):
-            who = source_of(j)
-            arrived(target, landed, who)
-            into[...] += target[who].astype(F32)
-
-        loop(count, step)
+    def spread(order, target, one_sem, two_sem, slot):
+        first, second = order, "y" if order == "x" else "x"
+        me, size, place = rings[first]
+        then, others, then_place = rings[second]
+        mine = then * size + me
+        line = target.at[pl.ds(then * size, size)]
+
+        def start():
+            for p in around(first):
+                push(target.at[mine], target, mine, send_sem.at[slot], one_sem, place(p))
+
+        def forward():
+            all_of(target.at[pl.ds(0, size - 1)], one_sem)
+            for q in around(second):
+                pltpu.make_async_remote_copy(
+                    src_ref=line,
+                    dst_ref=line,
+                    send_sem=send_sem.at[slot + 1],
+                    recv_sem=two_sem,
+                    device_id=then_place(q),
+                    device_id_type=MESH,
+                ).start()
+
+        def finish():
+            all_of(target.at[pl.ds(0, (others - 1) * size)], two_sem)
+
+        return mine, start, forward, finish
+
+    def add_up(target, landed, into):
+        all_of(target, landed)
+        sums = target[0].astype(F32)
+        for k in range(1, target.shape[0]):
+            sums += target[k].astype(F32)
+        into[...] = sums
 
     def factor(sq_r, q_sem):
-        def step(j, sums):
-            who = kv_source(j)
-            arrived(sq_r, q_sem, who)
-            return sums + sq_r[who]
-
-        sums = lax.fori_loop(0, n, step, jnp.zeros((1, 128), F32))
+        all_of(sq_r, q_sem)
+        sums = jnp.zeros((1, 128), F32)
+        for k in range(n):
+            sums += sq_r[k]
         row = lax.rsqrt(sums * (1.0 / width) + EPS)
         return jnp.transpose(jnp.broadcast_to(row, (128, 128)))[0:rows]
 
     def back(gs, weight, o, p, p_sem, p_slot, m, s, r, r_sem, r_slot):
         def multiply(i):
             chip = z_far(i)
-            pair = pl.ds(chip * 2, 2)
-            product = None
-            for g, landed, first in gs:
-                arrived(g, landed, chip * 2)
-                arrived(g, landed, chip * 2 + 1)
-                size = g.shape[2]
-                term = jnp.dot(
-                    g[pair].reshape(2 * rows, size),
-                    weight[pl.ds(first, size), :],
-                    preferred_element_type=F32,
-                )
-                product = term if product is None else product + term
+            lefts = []
+            for g, order in gs:
+                if order == "y":
+                    at = chip * 2 % nx * ny + chip * 2 // nx
+                    left = jnp.concatenate((g[at], g[at + ny]), axis=0)
+                else:
+                    left = g[pl.ds(chip * 2, 2)].reshape(2 * rows, g.shape[2])
+                lefts.append(left)
+            product = jnp.dot(
+                jnp.concatenate(lefts, axis=1), weight[...], preferred_element_type=F32
+            )
             low, high = product[0:rows], product[rows : 2 * rows]
             o[chip] = jnp.where(core == 0, high, low).astype(BF16)
-            push(o.at[chip], p, chip, send_sem.at[p_slot], p_sem, (kv, mate))
+            push(o.at[chip], p, chip, send_sem.at[p_slot], p_sem.at[chip], (kv, mate))
             m[chip] = jnp.where(core == 0, low, high)
 
         def pass_on(i):
@@ -354,27 +401,26 @@
 
             @pl.when(chip == z)
             def _():
-                pltpu.make_async_copy(s.at[chip], r.at[z], r_sem.at[z]).start()
+                pltpu.make_async_copy(s.at[chip], r.at[z], r_sem).start()
 
         loop(nz, multiply)
         loop(nz, pass_on)
-        drains.append((p, nz, p_slot))
-        drains.append((r, nz - 1, r_slot))
+        drains.append((p, p_slot))
+        drains.append((r.at[pl.ds(0, nz - 1)], r_slot))
 
     gather_tp(tokens, x1, 0, x1_sem)
-    for copy in loads[0:n_mix]:
-        copy.wait()
+    all_of(w_mix, w_sem.at[0])
     orders = ["x", "y"] * heads
     send_squares = projected(
-        x1, x1_sem, 0, mix_gain, w_mix, s2, orders, sq_s2, sq_r2, q2_sem, 1
+        x1, x1_sem, 0, mix_gain, w_mix, s2, orders, None, sq_s2, sq_r2, q2_sem, 1
     )
     stages = [
-        two_stages(order, c, s2, t2, u2, v2, t2_sem, v2_sem, 2 + 2 * c)
+        two_stages(order, c, s2, t2, u2, v2, t2_sem, v2_sem, 2)
         for c, order in enumerate(orders)
     ]
+    send_squares()
     for start, _, _ in stages:
         start()
-    send_squares()
     for _, middle, _ in stages:
         middle()
 
@@ -394,11 +440,8 @@
         values[:, at] = value
         kept = query * forget
         added = jnp.sum(query - kept, axis=-1, keepdims=True) * value
-        acc2[:, 0:HEAD] = kept
-
-        def eight(group, carry):
-            eight_rows = pl.ds(pl.multiple_of(group * 8, 8), 8)
-            columns = jnp.transpose(acc2[eight_rows, 0:HEAD])
+        for group in range(rows // 8):
+            columns = jnp.transpose(kept[group * 8 : (group + 1) * 8])
             reads = []
             for b in range(8):
                 reads.append(
@@ -406,35 +449,36 @@
                         columns[:, b : b + 1] * state[group * 8 + b, h], axis=0, keepdims=True
                     )
                 )
-            total[eight_rows, 0:HEAD] = jnp.concatenate(reads, axis=0)
-            return carry
-
-        lax.fori_loop(0, rows // 8, eight, 0)
+            total[group * 8 : (group + 1) * 8, 0:HEAD] = jnp.concatenate(reads, axis=0)
         read = total[:, 0:HEAD] + added
         mean = jnp.mean(read * read, axis=-1, keepdims=True)
         read = read * lax.rsqrt(mean + EPS) * head_gain[...]
         gated[h] = (read * (gate * jax.nn.sigmoid(gate))).astype(BF16)
-        gather_kv(gated.at[h], (g3a, g3b)[h], (10, 11)[h], (g3a_sem, g3b_sem)[h])
-
-    loads[n_mix].wait()
-    back([(g3a, g3a_sem, 0), (g3b, g3b_sem, HEAD)], w_out, o4, p4, p4_sem, 12, m4, s4, r4, r4_sem, 13)
-    add_up(nz, z_near, r4, r4_sem, total)
+        gather_kv(gated.at[h], g3.at[h], send_sem.at[4], g3_sem.at[h])
+
+    all_of(w_out, w_sem.at[1])
+    for h in range(heads):
+        all_of(g3.at[h], g3_sem.at[h])
+    back([(g3.at[h], "x") for h in range(heads)], w_out, o4, p4, p4_sem, 5, m4, s4, r4, r4_sem, 6)
+    add_up(r4, r4_sem, total)
     own[...] = (tokens[...].astype(F32) + total[...]).astype(BF16)
 
-    gather_tp(own, x5, 14, x5_sem)
-    for copy in loads[n_mix + 1 : -1]:
-        copy.wait()
-    orders = [("x", "y")[c % 2] for c in range(units - 1)] + ["direct"]
+    gather_tp(own, x5, 7, x5_sem)
+    all_of(w_ffn, w_sem.at[2])
+    orders = [("x", "y")[c % 2] for c in range(units - 1)] + ["both"]
     send_squares = projected(
-        x5, x5_sem, 14, ffn_gain, w_ffn, s6, orders, sq_s6, sq_r6, q6_sem, 15
+        x5, x5_sem, 7, ffn_gain, w_ffn, s6, orders, s7, sq_s6, sq_r6, q6_sem, 8
     )
     stages = [
-        two_stages(order, c, s6, t6, u6, v6, t6_sem, v6_sem, 16 + 2 * c)
+        two_stages(order, c, s6, t6, u6, v6, t6_sem, v6_sem, 9)
         for c, order in enumerate(orders[:-1])
     ]
-    for start, _, _ in stages:
+    stages += [
+        two_stages("xy"[c], c, s7, t7, u7, v7, t7_sem, v7_sem, 11) for c in range(2)
+    ]
+    send_squares()
+    for start, _, _ in stages[: units - 1]:
         start()
-    send_squares()
 
     def renew(group, carry):
         first = pl.multiple_of(group * 8, 8)
@@ -448,37 +492,68 @@
         return carry
 
     lax.fori_loop(0, rows // 8, renew, 0)
+    state_store = pltpu.make_async_copy(state, state_out, so_sem)
+    state_store.start()
     stages[0][1]()
     stages[1][1]()
-    direct = s6.at[units - 1]
-    loop(n, lambda j: to_kv(direct.at[kv_peer(j)], d6, send_sem.at[24], d6_sem, kv_peer(j)))
-    drains.append((d6, n - 1, 24))
-    for _, middle, _ in stages[2:]:
+    for start, _, _ in stages[units - 1 :]:
+        start()
+    for _, middle, _ in stages[2 : units - 1]:
         middle()
     scale = factor(sq_r6, q6_sem)
 
-    def activate(sums, hid, c):
-        gate, upper = sums[:, 0:HEAD] * scale, sums[:, HEAD:WIDE] * scale
-        hid[:, c * HEAD : (c + 1) * HEAD] = (gate * jax.nn.sigmoid(gate) * upper).astype(BF16)
-
-    early = 2
-    for c in range(early):
-        activate(stages[c][2](), hida, c)
-    gather_kv(hida, h7a, 25, h7a_sem)
-    for c in range(early, units - 1):
-        activate(stages[c][2](), hidb, c - early)
-    add_up(n, kv_source, d6, d6_sem, acc6)
-    activate(acc6[...], hidb, units - 1 - early)
-    gather_kv(hidb, h7b, 26, h7b_sem)
-    loads[-1].wait()
-    gs = [(h7a, h7a_sem, 0), (h7b, h7b_sem, early * HEAD)]
-    back(gs, w_down, o8, p8, p8_sem, 27, m8, s8, r8, r8_sem, 28)
-    add_up(nz, z_near, r8, r8_sem, total)
+    def activated(gate, upper):
+        gate, upper = gate * scale, upper * scale
+        return (gate * jax.nn.sigmoid(gate) * upper).astype(BF16)
+
+    spreads = [
+        spread(order, h7.at[c], h7_sem.at[c], h7_line_sem.at[c], 13)
+        for c, order in enumerate(orders[:-1])
+    ]
+
+    def share(c):
+        mine, start, _, _ = spreads[c]
+        sums = stages[c][2]()
+        h7[c, mine] = activated(sums[:, 0:HEAD], sums[:, HEAD:WIDE])
+        start()
+
+    share(0)
+    share(1)
+    for _, middle, _ in stages[units - 1 :]:
+        middle()
+    for c in range(2, units - 1):
+        share(c)
+    for _, _, forward, _ in spreads[:2]:
+        forward()
+    hidden[...] = activated(stages[units - 1][2](), stages[units][2]())
+    gather_kv(hidden, h7c, send_sem.at[15], h7c_sem)
+    for _, _, forward, _ in spreads[2:]:
+        forward()
+    for _, _, _, finish in spreads:
+        finish()
+    groups = [(h7.at[c], orders[c]) for c in range(units - 1)] + [(h7c, "x")]
+    all_of(h7c, h7c_sem)
+    all_of(w_down, w_sem.at[3])
+    back(groups, w_down, o8, p8, p8_sem, 16, m8, s8, r8, r8_sem, 17)
+    add_up(r8, r8_sem, total)
     out[...] = (own[...].astype(F32) + total[...]).astype(BF16)
 
-    for target, count, slot in drains:
-        sent = target.at[pl.ds(0, count)]
-        pltpu.make_async_copy(sent, sent, send_sem.at[slot]).wait()
+    state_store.wait()
+    last = nx - 1
+    drains += [
+        (t2.at[:, pl.ds(0, last)], 2),
+        (v2.at[:, pl.ds(0, last)], 3),
+        (g3.at[:, pl.ds(0, n - 1)], 4),
+        (t6.at[:, pl.ds(0, last)], 9),
+        (v6.at[:, pl.ds(0, last)], 10),
+        (t7.at[:, pl.ds(0, last)], 11),
+        (v7.at[:, pl.ds(0, last)], 12),
+        (h7.at[:, pl.ds(0, last)], 13),
+        (h7.at[:, pl.ds(0, last * nx)], 14),
+        (h7c.at[pl.ds(0, n - 1)], 15),
+    ]
+    for sent, slot in drains:
+        all_of(sent, send_sem.at[slot])
 
 
 def publish(rows_in, state_in, rows_out, state_out, sem):
@@ -515,6 +590,7 @@
     vmem, dma = pltpu.VMEM, pltpu.SemaphoreType.DMA
     in_vmem = pl.BlockSpec(memory_space=pltpu.VMEM)
     in_hbm = pl.BlockSpec(memory_space=pltpu.HBM)
+    in_place = pl.BlockSpec(memory_space=pl.ANY)
     block = (rows, cols)
     all_blocks = vmem((n, *block), BF16)
     chip_blocks = vmem((nz, *block), BF16)
@@ -523,7 +599,7 @@
     ny, wide = n // nx, 2 * HEAD
     units, mixed = up // HEAD, 2 * (side // HEAD)
 
-    def staged(chunks):
+    def staged(chunks, wide=wide):
         return [
             vmem((chunks, nx, ny, rows, wide), BF16),
             vmem((chunks, nx, rows, wide), BF16),
@@ -537,9 +613,15 @@
             pltpu.VMEM(block, BF16),
             pltpu.VMEM(state.shape, F32),
         ),
-        in_specs=[in_vmem, in_hbm, in_vmem, in_vmem, in_vmem, in_vmem] + [in_hbm] * 8,
-        out_specs=(in_vmem, in_vmem),
+        in_specs=[in_hbm] * 14,
+        out_specs=(in_vmem, in_place),
         scratch_shapes=[
+            vmem(state.shape, F32),
+            vmem(block, BF16),
+            vmem((1, cols), F32),
+            vmem((1, side), F32),
+            vmem((1, HEAD), F32),
+            vmem((1, cols), F32),
             vmem((cols, 4 * side), BF16),
             vmem(out_weight.shape, BF16),
             vmem((cols, 2 * up), BF16),
@@ -554,42 +636,43 @@
             vmem((rows, 4 * HEAD), F32),
             vmem(block, F32),
             vmem((side // HEAD, rows, HEAD), BF16),
-            vmem((n, rows, HEAD), BF16),
-            vmem((n, rows, HEAD), BF16),
+            vmem((side // HEAD, n, rows, HEAD), BF16),
             *backward,
             vmem(block, BF16),
             all_blocks,
-            vmem((units, n, rows, wide), BF16),
+            vmem((units - 1, n, rows, wide), BF16),
             *staged(units - 1),
-            vmem((n, rows, wide), BF16),
+            vmem((2, n, rows, HEAD), BF16),
+            *staged(2, HEAD),
             squares,
             squares,
-            vmem((rows, wide), F32),
-            vmem((rows, 2 * HEAD), BF16),
-            vmem((rows, up - 2 * HEAD), BF16),
-            vmem((n, rows, 2 * HEAD), BF16),
-            vmem((n, rows, up - 2 * HEAD), BF16),
+            vmem((rows, HEAD), BF16),
+            vmem((units - 1, n, rows, HEAD), BF16),
+            vmem((n, rows, HEAD), BF16),
             *backward,
-            dma((2 * mixed + 2 * units + 2,)),
+            dma((5,)),
+            dma((4,)),
             dma,
-            dma((29,)),
+            dma,
+            dma((18,)),
             dma((n,)),
-            dma((mixed, nx)),
-            dma((mixed, nx)),
+            dma((mixed,)),
+            dma((mixed,)),
+            dma,
+            dma((side // HEAD,)),
+            dma((nz,)),
+            dma,
             dma((n,)),
-            dma((n,)),
-            dma((n,)),
+            dma((units - 1,)),
+            dma((units - 1,)),
+            dma((2,)),
+            dma((2,)),
+            dma,
+            dma((units - 1,)),
+            dma((units - 1,)),
+            dma,
             dma((nz,)),
-            dma((nz,)),
-            dma((n,)),
-            dma((units - 1, nx)),
-            dma((units - 1, nx)),
-            dma((n,)),
-            dma((n,)),
-            dma((n,)),
-            dma((n,)),
-            dma((nz,)),
-            dma((nz,)),
+            dma,
         ],
         compiler_params=pltpu.CompilerParams(
             collective_id=0, has_side_effects=True, vmem_limit_bytes=57 * 2**20
@@ -617,7 +700,7 @@
             jax.ShapeDtypeStruct(block, BF16),
             jax.ShapeDtypeStruct(state.shape, F32),
         ),
-        in_specs=[in_vmem, in_vmem],
+        in_specs=[in_place, in_place],
         out_specs=(in_hbm, in_hbm),
         scratch_shapes=[dma((rows // 4 + 1,))],
         compiler_params=pltpu.CompilerParams(vmem_limit_bytes=8 * 2**20),

time: 92.7 us -> 89.4 us (0.964)
  Pallas kernels: 91.9 us -> 88.7 us
    pallas_call x1, Pallas kernels: 89.5 us -> 86.3 us  [body(): pl.pallas_call(functools.partial(layer, n, nx, nz, cols * n), out_shape=(...]
where the time goes in v6:
time: 89.4 us
  Pallas kernels  88.7 us (99%)
    pallas_call x1, Pallas kernels, body(): pl.pallas_call(functools.partial(layer, n, nx, nz, cols * n), out_shape=(...  86.3 us
    pallas_call x1, Pallas kernels, body(): pl.pallas_call(publish, out_shape=(jax.ShapeDtypeStruct(block, BF16), jax...  2.43 us

profile of v6, /device:TPU:1, one launch (start us, length us, event | category | flops | bytes accessed | tf_op | source)
XLA Modules:
  0.0 89.4 jit_solution(3787295294685378779)
XLA Ops:
  0.6 86.3 %layer.1 = (bf16[40,256]{1,0:T(8,128)(2,1)S(1)}, f32[40,2,128,128]{3,2,1,0:T(8,128)S(1)}) custom-call(bf16[40,256]{1,0:T(8,128)(2,1)} %refs_0_.1, f32[40,2,128,128]{3,2,1,0:T(8,128)} %refs_1_.1, f32[1,256]{1,0:T(1,128)} %bitcast.4, f32[1,256]{1,0:T(1,128)} %bitcast.5, f32[1,128]{1,0:T(1,128)} %bitcast.7, f32[1,256]{1,0:T(1,128)} %bitcast.6, ...), custom_call_target="tpu_custom_call" | custom-call | tf_op jit(solution)/shard_map/layer/pallas_call | solution.py:610
  86.9 2.4 %publish.1 = (bf16[40,256]{1,0:T(8,128)(2,1)}, f32[40,2,128,128]{3,2,1,0:T(8,128)}) custom-call(bf16[40,256]{1,0:T(8,128)(2,1)S(1)} %get-tuple-element.4.rows_in, f32[40,2,128,128]{3,2,1,0:T(8,128)S(1)} %get-tuple-element.5.state_in), custom_call_target="tpu_custom_call" | custom-call | tf_op jit(solution)/shard_map/publish/pallas_call | solution.py:697

commit v7 on v6

--- a/solution.py
+++ b/solution.py
@@ -54,7 +54,6 @@
         v2,
         sq_s2,
         sq_r2,
-        acc2,
         total,
         gated,
         g3,
@@ -145,8 +144,7 @@
         (ffn_gain_in, ffn_gain),
     )
     smalls = [pltpu.make_async_copy(a, b, small_sem.at[i]) for i, (a, b) in enumerate(smalls)]
-    for copy in smalls:
-        copy.start()
+    smalls[0].start()
     barrier = pltpu.get_barrier_semaphore()
 
     def greet(who):
@@ -168,10 +166,8 @@
 
     loads = []
     for h in range(heads):
-        for k, w in enumerate((wq_in, wf_in, wi_in, wg_in)):
-            loads.append(
-                (w.at[:, pl.ds(h * HEAD, HEAD)], w_mix.at[:, pl.ds((4 * h + k) * HEAD, HEAD)])
-            )
+        for w, c in ((wq_in, 2 * h), (wf_in, 2 * h + 1), (wi_in, 2 * heads + h), (wg_in, 3 * heads + h)):
+            loads.append((w.at[:, pl.ds(h * HEAD, HEAD)], w_mix.at[:, pl.ds(c * HEAD, HEAD)]))
     n_mix = len(loads)
     loads.append((wo_in, w_out))
     units = up // HEAD
@@ -183,13 +179,10 @@
     loads.append((wfd_in, w_down))
     kinds = [0] * n_mix + [1] + [2] * (2 * units) + [3]
     loads = [pltpu.make_async_copy(a, b, w_sem.at[k]) for k, (a, b) in zip(kinds, loads)]
-    for copy in loads:
-        copy.start()
     state_load = pltpu.make_async_copy(state_in, state, st_sem)
-    state_load.start()
+
     pl.semaphore_wait(barrier, (n - 1) + (nz - 1) + 1)
-    for copy in smalls:
-        copy.wait()
+    smalls[0].wait()
 
     def push(source, target, where, sent, landed, device):
         pltpu.make_async_remote_copy(
@@ -232,7 +225,7 @@
         drains.append((target.at[pl.ds(0, n - 1)], slot))
 
     def projected(x, x_sem, x_slot, gain, weight, s, orders, halves, sq_s, sq_r, q_sem, q_slot):
-        ones = jnp.ones((8, cols), F32)
+        ones = jnp.ones((8, 2 * cols), BF16)
         lag = min(2, nz)
         sq_s[...] = jnp.zeros_like(sq_s)
 
@@ -265,11 +258,13 @@
                             halves[1, y_at] = part[:, HEAD:WIDE]
                         else:
                             s[c, x_at if order == "x" else y_at] = part
+                squares = values * values
+                high = squares.astype(BF16)
+                rest = (squares - high.astype(F32)).astype(BF16)
                 squares = lax.dot_general(
                     ones,
-                    values * values,
+                    jnp.concatenate((high, rest), axis=1),
                     (((1,), (1,)), ((), ())),
-                    precision=lax.Precision.HIGHEST,
                     preferred_element_type=F32,
                 )
                 for k in range(2):
@@ -409,6 +404,11 @@
         drains.append((r.at[pl.ds(0, nz - 1)], r_slot))
 
     gather_tp(tokens, x1, 0, x1_sem)
+    for copy in smalls[1:] + loads:
+        copy.start()
+    state_load.start()
+    for copy in smalls[1:]:
+        copy.wait()
     all_of(w_mix, w_sem.at[0])
     orders = ["x", "y"] * heads
     send_squares = projected(
@@ -426,40 +426,53 @@
 
     scale = factor(sq_r2, q2_sem)
     state_load.wait()
+    added = []
+    row_of_eight = lax.broadcasted_iota(jnp.int32, (8, HEAD), 0)
     for h in range(heads):
         at = pl.ds(h * HEAD, HEAD)
-        acc2[:, 0:WIDE] = stages[2 * h][2]()
-        acc2[:, WIDE : 2 * WIDE] = stages[2 * h + 1][2]()
-        query = acc2[:, 0:HEAD] * scale
+        sums = stages[h][2]()
+        query = sums[:, 0:HEAD] * scale
         query = query * jax.nn.sigmoid(query) * (HEAD ** (-0.5))
         low = lower_bound[:, at]
-        forget = low + (1.0 - low) * jax.nn.sigmoid(acc2[:, HEAD : 2 * HEAD] * scale)
-        value = acc2[:, 2 * HEAD : 3 * HEAD] * scale
-        gate = acc2[:, 3 * HEAD : 4 * HEAD] * scale
+        forget = low + (1.0 - low) * jax.nn.sigmoid(sums[:, HEAD:WIDE] * scale)
         forgets[:, at] = forget
+        kept = query * forget
+        added.append(jnp.sum(query - kept, axis=-1, keepdims=True))
+        kept_high = kept.astype(BF16)
+        kept_low = (kept - kept_high.astype(F32)).astype(BF16)
+        for group in range(rows // 8):
+            eight = slice(group * 8, (group + 1) * 8)
+            left = jnp.concatenate(
+                (kept_high[eight].astype(F32), kept_low[eight].astype(F32)), axis=0
+            ).astype(BF16)
+            left = jnp.concatenate((left, left), axis=1)
+            reads = jnp.zeros((8, HEAD), F32)
+            for b in range(8):
+                right = state[group * 8 + b, h]
+                high = right.astype(BF16)
+                rest = (right - high.astype(F32)).astype(BF16)
+                product = jnp.dot(
+                    left, jnp.concatenate((high, rest), axis=0), preferred_element_type=F32
+                )
+                reads = jnp.where(row_of_eight == b, product[0:8] + product[8:16], reads)
+            total[eight, at] = reads
+    value_sums = stages[heads][2]()
+    gate_sums = stages[heads + 1][2]()
+    for h in range(heads):
+        at = pl.ds(h * HEAD, HEAD)
+        part = slice(h * HEAD, (h + 1) * HEAD)
+        value = value_sums[:, part] * scale
+        gate = gate_sums[:, part] * scale
         values[:, at] = value
-        kept = query * forget
-        added = jnp.sum(query - kept, axis=-1, keepdims=True) * value
-        for group in range(rows // 8):
-            columns = jnp.transpose(kept[group * 8 : (group + 1) * 8])
-            reads = []
-            for b in range(8):
-                reads.append(
-                    jnp.sum(
-                        columns[:, b : b + 1] * state[group * 8 + b, h], axis=0, keepdims=True
-                    )
-                )
-            total[group * 8 : (group + 1) * 8, 0:HEAD] = jnp.concatenate(reads, axis=0)
-        read = total[:, 0:HEAD] + added
+        read = total[:, at] + added[h] * value
         mean = jnp.mean(read * read, axis=-1, keepdims=True)
         read = read * lax.rsqrt(mean + EPS) * head_gain[...]
-        gated[h] = (read * (gate * jax.nn.sigmoid(gate))).astype(BF16)
-        gather_kv(gated.at[h], g3.at[h], send_sem.at[4], g3_sem.at[h])
+        gated[:, at] = (read * (gate * jax.nn.sigmoid(gate))).astype(BF16)
+    gather_kv(gated, g3, send_sem.at[4], g3_sem)
 
     all_of(w_out, w_sem.at[1])
-    for h in range(heads):
-        all_of(g3.at[h], g3_sem.at[h])
-    back([(g3.at[h], "x") for h in range(heads)], w_out, o4, p4, p4_sem, 5, m4, s4, r4, r4_sem, 6)
+    all_of(g3, g3_sem)
+    back([(g3, "x")], w_out, o4, p4, p4_sem, 5, m4, s4, r4, r4_sem, 6)
     add_up(r4, r4_sem, total)
     own[...] = (tokens[...].astype(F32) + total[...]).astype(BF16)
 
@@ -543,7 +556,7 @@
     drains += [
         (t2.at[:, pl.ds(0, last)], 2),
         (v2.at[:, pl.ds(0, last)], 3),
-        (g3.at[:, pl.ds(0, n - 1)], 4),
+        (g3.at[pl.ds(0, n - 1)], 4),
         (t6.at[:, pl.ds(0, last)], 9),
         (v6.at[:, pl.ds(0, last)], 10),
         (t7.at[:, pl.ds(0, last)], 11),
@@ -633,10 +646,9 @@
             *staged(mixed),
             squares,
             squares,
-            vmem((rows, 4 * HEAD), F32),
             vmem(block, F32),
-            vmem((side // HEAD, rows, HEAD), BF16),
-            vmem((side // HEAD, n, rows, HEAD), BF16),
+            vmem((rows, side), BF16),
+            vmem((n, rows, side), BF16),
             *backward,
             vmem(block, BF16),
             all_blocks,
@@ -659,7 +671,7 @@
             dma((mixed,)),
             dma((mixed,)),
             dma,
-            dma((side // HEAD,)),
+            dma,
             dma((nz,)),
             dma,
             dma((n,)),

time: 89.4 us -> 88.4 us (0.989)
  Pallas kernels: 88.7 us -> 87.7 us
    pallas_call x1, Pallas kernels: 86.3 us -> 85.2 us  [body(): pl.pallas_call(functools.partial(layer, n, nx, nz, cols * n), out_shape=(...]
where the time goes in v7:
time: 88.4 us; the launch traced here: 88.3 us
  Pallas kernels  87.7 us (99%)
    pallas_call x1, Pallas kernels, body(): pl.pallas_call(functools.partial(layer, n, nx, nz, cols * n), out_shape=(...  85.2 us
    pallas_call x1, Pallas kernels, body(): pl.pallas_call(publish, out_shape=(jax.ShapeDtypeStruct(block, BF16), jax...  2.43 us

profile of v7, /device:TPU:1, one launch (start us, length us, event | category | flops | bytes accessed | tf_op | source)
XLA Modules:
  0.0 88.3 jit_solution(9117377038220110183)
XLA Ops:
  0.6 85.2 %layer.1 = (bf16[40,256]{1,0:T(8,128)(2,1)S(1)}, f32[40,2,128,128]{3,2,1,0:T(8,128)S(1)}) custom-call(bf16[40,256]{1,0:T(8,128)(2,1)} %refs_0_.1, f32[40,2,128,128]{3,2,1,0:T(8,128)} %refs_1_.1, f32[1,256]{1,0:T(1,128)} %bitcast.4, f32[1,256]{1,0:T(1,128)} %bitcast.5, f32[1,128]{1,0:T(1,128)} %bitcast.7, f32[1,256]{1,0:T(1,128)} %bitcast.6, ...), custom_call_target="tpu_custom_call" | custom-call | tf_op jit(solution)/shard_map/layer/pallas_call | solution.py:623
  85.9 2.4 %publish.1 = (bf16[40,256]{1,0:T(8,128)(2,1)}, f32[40,2,128,128]{3,2,1,0:T(8,128)}) custom-call(bf16[40,256]{1,0:T(8,128)(2,1)S(1)} %get-tuple-element.4.rows_in, f32[40,2,128,128]{3,2,1,0:T(8,128)S(1)} %get-tuple-element.5.state_in), custom_call_target="tpu_custom_call" | custom-call | tf_op jit(solution)/shard_map/publish/pallas_call | solution.py:709
